TPU v7x, 32 devices: a whole 2x2x4 slice. The times are simulated.
32 devices in a mesh: sp: 8 (over z, y), tp: 4 (over x, core).
Axes of the slice: x: 2, y: 2, z: 4, core: 2. Of those that a mesh axis runs over, the one named last changes fastest.
Arguments:
- stream: bfloat16 [16384, 4096], P('sp', 'tp'), may hold values from -18 to 18
- doc_ids: int32 [16384], P('sp'), may hold values from 0 to 1, never falling along the last dimension, each value on 1 to 12288 neighbouring positions
- norm_gain: bfloat16 [3, 4096], replicated, may hold values from 0.099609375 to 1.8984375
- proj_in: bfloat16 [3, 4096, 1024], P(None, 'tp', 'sp'), may hold values from -0.09375 to 0.09375
- mix_pool: bfloat16 [3, 8, 128, 128], replicated, may hold values from -0.5 to 0.5
- pool_gain: bfloat16 [3, 1024], replicated, may hold values from 0.099609375 to 1.8984375
- proj_out: bfloat16 [3, 1024, 4096], P(None, 'sp', 'tp'), may hold values from -0.1875 to 0.1875
Outputs:
- stream_out: bfloat16 [16384, 4096], P('sp', 'tp')
Inputs may be any that keep to these rules, and one draw needn't show every extreme that they name: `doc_ids`: document numbers never fall along the sequence; each document holds 1 to 12288 positions, one exactly that many.
All inputs are finite; a program needn't handle non-finite values.
Results may differ from a plain program's by a relative error of at most 0.02.
Values may be sent and summed in bfloat16 or wider, within the bound.
A program may use at most 64 MiB of HBM per device.

v0:
```python
import functools

import jax
import jax.numpy as jnp
from jax import lax
from jax.experimental import pallas as pl
from jax.experimental.pallas import tpu as pltpu
from jax.sharding import PartitionSpec as P

EPSILON = 1e-06
HALO = 16
CHUNKS = 8
LAG = 4
MESH = pl.DeviceIdType.MESH
F32, BF16 = jnp.float32, jnp.bfloat16


def mixer(sp, tp, snake, x_ref, doc_ref, gains_ref, win_ref, mix_ref, pgains_ref, wout_ref, o_ref,
          win, wout, send1, own1, recv1, sum2, recv2, mixed, zbuf, hrecv,
          sq_own, sq_in1, sq_sum, sq_in2,
          labels, before_labels, pos_ref, gain_ref, pgain_ref, ls, lr,
          ring_s, ring_r, s1, r1, s2, r2, s3, r3, hs, hr):
    layers, model_dev, chan_dev = win_ref.shape
    tokens = x_ref.shape[0]
    rows = tokens // CHUNKS
    channels = chan_dev * sp
    half = channels // 2
    group = mix_ref.shape[-1]
    model = model_dev * tp
    row_dev = wout_ref.shape[1]
    s, t = lax.axis_index("sp"), lax.axis_index("tp")
    core = lax.rem(t, 2)
    partner = t + 1 - 2 * core
    across = lax.rem(t + 2, tp)

    def place(device):
        if not snake:
            return device
        z, y = device // 2, lax.rem(device, 2)
        return z * (1 - y) + (sp - 1 - z) * y

    def device_at(place):
        if not snake:
            return place
        up = place // (sp // 2)
        return 2 * (place * (1 - up) + (sp - 1 - place) * up) + up

    here = place(s)
    after, before = device_at(lax.rem(here + 1, sp)), device_at(lax.rem(here + sp - 1, sp))
    following, leading = lax.rem(s + 1, sp), lax.rem(s + sp - 1, sp)

    barrier = pltpu.get_barrier_semaphore()
    for peer in ({"tp": partner}, {"tp": across}, {"sp": after}, {"sp": before}, {"sp": following}, {"sp": leading}):
        pl.semaphore_signal(barrier, inc=1, device_id=peer, device_id_type=MESH)
    pl.semaphore_wait(barrier, 6)

    ahead = sp // 2

    def hops(way, piece):
        return ahead if way == piece else ahead - 1

    def ring_view(layer, side, piece, source, own):
        if side == 0:
            part = model_dev // 2
            cut = pl.ds(piece * part, part)
            target = win.at[layer, cut, pl.ds(pl.multiple_of(source * chan_dev, chan_dev), chan_dev)]
            return (win_ref.at[layer, cut] if own else target), target
        part = row_dev // 2
        target = wout.at[layer, pl.ds(pl.multiple_of(source * row_dev + piece * part, part), part)]
        return (wout_ref.at[layer, pl.ds(piece * part, part)] if own else target), target

    def ring_copy(layer, side, piece, way, hop, own):
        origin = here - hop + sp if way == 0 else here + hop
        source = device_at(lax.rem(origin, sp))
        src, dst = ring_view(layer, side, piece, source, own)
        return pltpu.make_async_remote_copy(
            src_ref=src, dst_ref=dst,
            send_sem=ring_s.at[layer, side, piece, way, hop], recv_sem=ring_r.at[layer, side, piece, way, hop],
            device_id={"sp": after if way == 0 else before}, device_id_type=MESH)

    def ring_land(layer, side, piece, way, hop):
        origin = here - hop - 1 + 2 * sp if way == 0 else here + hop + 1
        _, dst = ring_view(layer, side, piece, device_at(lax.rem(origin, sp)), False)
        return pltpu.make_async_remote_copy(
            src_ref=dst, dst_ref=dst,
            send_sem=ring_s.at[layer, side, piece, way, hop], recv_sem=ring_r.at[layer, side, piece, way, hop],
            device_id={"sp": after if way == 0 else before}, device_id_type=MESH)

    def ring_start(layer, side, piece):
        for way in range(2):
            if hops(way, piece) > 0:
                ring_copy(layer, side, piece, way, 0, True).start()

    def ring_step(layer, side, piece, hop):
        for way in range(2):
            @pl.when(hop < hops(way, piece))
            def _():
                ring_land(layer, side, piece, way, hop).wait_recv()

            @pl.when(hop + 1 < hops(way, piece))
            def _():
                ring_copy(layer, side, piece, way, hop + 1, False).start()

    item_count = 2 * layers
    per_step = -(-ahead // (CHUNKS // 2))
    item_steps = -(-ahead // per_step)

    def pump(step, piece):
        item = 1 + step // item_steps
        layer, side = item // 2, lax.rem(item, 2)

        @pl.when(item < item_count)
        def _():
            for which in range(2):
                @pl.when(side == which)
                def _():
                    for j in range(per_step):
                        hop = lax.rem(step, item_steps) * per_step + j
                        if ahead % per_step == 0:
                            ring_step(layer, which, piece, hop)
                        else:
                            @pl.when(hop < ahead)
                            def _():
                                ring_step(layer, which, piece, hop)

        following_item = item + 1

        @pl.when((following_item < item_count) & (lax.rem(step, item_steps) == max(item_steps - 2, 0)))
        def _():
            for which in range(2):
                @pl.when(lax.rem(following_item, 2) == which)
                def _():
                    ring_start(following_item // 2, which, piece)

    for piece in range(2):
        ring_start(0, 0, piece)
    reach = 2 * HALO
    documents = doc_ref[...].astype(F32)
    for j in range(tokens // 128):
        labels[pl.ds(reach + j * 128, 128)] = jnp.broadcast_to(documents[j:j + 1], (128, 128)).T
    label_copy = pltpu.make_async_remote_copy(
        src_ref=labels.at[pl.ds(tokens, reach)], dst_ref=before_labels, send_sem=ls, recv_sem=lr,
        device_id={"sp": following}, device_id_type=MESH)
    label_copy.start()
    for layer in range(layers):
        win[layer, :, pl.ds(pl.multiple_of(s * chan_dev, chan_dev), chan_dev)] = win_ref[layer]
        wout[layer, pl.ds(pl.multiple_of(s * row_dev, row_dev), row_dev), :] = wout_ref[layer]
        own_gain = gains_ref[:, pl.ds(pl.multiple_of(t * model_dev, model_dev), model_dev)].astype(F32)
        gain_ref[layer] = own_gain[layer:layer + 1]
        own_gain = pgains_ref[:, pl.ds(pl.multiple_of(core * half, half), half)].astype(F32)
        pgain_ref[layer] = own_gain[layer:layer + 1]

    def distances(ext):
        same = jnp.zeros((ext.shape[0] - HALO, 128), F32)
        for offset in range(1, HALO):
            same = same + (pltpu.roll(ext, offset, 0) == ext)[HALO:].astype(F32)
        return same

    label_copy.wait()
    labels[pl.ds(0, reach)] = jnp.where(s == 0, -1.0, before_labels[...])
    pos_ref[pl.ds(0, HALO)] = distances(labels[pl.ds(0, reach)])

    def prepare(i):
        at = pl.ds(pl.multiple_of(i * rows, rows), rows)
        o_ref[at] = x_ref[at]
        pos_ref[pl.ds(pl.multiple_of(HALO + i * rows, HALO), rows)] = distances(
            labels[pl.ds(pl.multiple_of(HALO + i * rows, HALO), rows + HALO)])

    @pl.loop(0, ahead)
    def _(hop):
        for piece in range(2):
            ring_step(0, 0, piece, hop)
            @pl.when(hop == max(ahead - 2, 0))
            def _():
                ring_start(0, 1, piece)

        share = -(-CHUNKS // ahead)
        for j in range(share):
            @pl.when(hop * share + j < CHUNKS)
            def _():
                prepare(hop * share + j)

    def split(step):
        layer = step // CHUNKS
        return layer, CHUNKS - 1 - lax.rem(step, CHUNKS)

    def copy1(i):
        return [pltpu.make_async_remote_copy(
            src_ref=a, dst_ref=b, send_sem=s1.at[j, i], recv_sem=r1.at[j, i],
            device_id={"tp": partner}, device_id_type=MESH)
            for j, (a, b) in enumerate(((send1.at[i], recv1.at[i]), (sq_own.at[i], sq_in1.at[i])))]

    def copy2(layer, i):
        par = lax.rem(layer, 2)
        return [pltpu.make_async_remote_copy(
            src_ref=a, dst_ref=b, send_sem=s2.at[j, i], recv_sem=r2.at[j, par, i],
            device_id={"tp": across}, device_id_type=MESH)
            for j, (a, b) in enumerate(((sum2.at[i], recv2.at[par, i]), (sq_sum.at[i], sq_in2.at[par, i])))]

    def copy3(i, side):
        view = mixed.at[i, :, pl.ds(pl.multiple_of(side * half, half), half)]
        return pltpu.make_async_remote_copy(
            src_ref=view, dst_ref=view, send_sem=s3.at[i], recv_sem=r3.at[i],
            device_id={"tp": partner}, device_id_type=MESH)

    def halo_copy(layer):
        return pltpu.make_async_remote_copy(
            src_ref=zbuf.at[pl.ds(tokens, HALO)], dst_ref=hrecv.at[layer], send_sem=hs.at[layer], recv_sem=hr.at[layer],
            device_id={"sp": following}, device_id_type=MESH)

    def project(step):
        layer, i = split(step)
        at = pl.ds(pl.multiple_of(i * rows, rows), rows)
        wide = o_ref[at].astype(F32)
        squares = wide * wide
        lanes = squares[:, :128]
        for j in range(1, model_dev // 128):
            lanes = lanes + squares[:, j * 128:(j + 1) * 128]
        sq_own[i] = jnp.sum(lanes.T.reshape(16, 8, rows), axis=0)
        gained = (wide * gain_ref[layer]).astype(BF16)
        other = pl.ds(pl.multiple_of((1 - core) * half, half), half)
        send1[i] = jnp.dot(gained, win[layer, :, other], preferred_element_type=F32).astype(BF16)
        for c in copy1(i):
            c.start()
        mine = pl.ds(pl.multiple_of(core * half, half), half)
        own1[i] = jnp.dot(gained, win[layer, :, mine], preferred_element_type=F32).astype(BF16)

    def join(step):
        layer, i = split(step)
        for c in copy1(i):
            c.wait()
        sum2[i] = (own1[i].astype(F32) + recv1[i].astype(F32)).astype(BF16)
        sq_sum[i] = sq_own[i] + sq_in1[i]
        for c in copy2(layer, i):
            c.start()

    def normalise(step):
        layer, i = split(step)
        par = lax.rem(layer, 2)
        for c in copy2(layer, i):
            c.wait()

        @pl.when(i == CHUNKS - 2)
        def _():
            halo_copy(layer).wait_send()

        total = jnp.sum(sq_sum[i] + sq_in2[par, i], axis=0, keepdims=True)
        scale = jnp.broadcast_to(lax.rsqrt(total / model + EPSILON), (128, rows)).T
        at = pl.ds(pl.multiple_of(HALO + i * rows, HALO), rows)
        for j in range(half // 128):
            cols = slice(j * 128, (j + 1) * 128)
            zbuf[at, cols] = ((sum2[i, :, cols].astype(F32) + recv2[par, i, :, cols].astype(F32)) * scale).astype(BF16)

        @pl.when(i == CHUNKS - 1)
        def _():
            halo_copy(layer).start()

    def pool(step):
        layer, i = split(step)

        @pl.when(i == 0)
        def _():
            halo_copy(layer).wait_recv()
            zbuf[pl.ds(0, HALO)] = hrecv[layer]

        wide_at = pl.ds(pl.multiple_of(i * rows, HALO), rows + HALO)
        pos = pos_ref[wide_at]
        for g in range(half // group):
            cols = slice(g * group, (g + 1) * group)
            z = zbuf[wide_at, cols].astype(F32)
            window = 2 ** (1 + g % 4)
            total = z
            step_rows = 1
            while step_rows < window:
                total = total + jnp.where(pos >= step_rows, pltpu.roll(total, step_rows, 0), 0.0)
                step_rows *= 2
            count = jnp.minimum(pos[HALO:] + 1.0, float(window))
            pooled = (total[HALO:] / count - z[HALO:]).astype(BF16)
            blended = jnp.dot(pooled, mix_ref[layer, core * (half // group) + g], preferred_element_type=F32)
            place_at = pl.ds(pl.multiple_of(core * half + g * group, group), group)
            mixed[i, :, place_at] = (blended * pgain_ref[layer, :, cols]).astype(BF16)
        copy3(i, core).start()

    def finish(step):
        layer, i = split(step)
        copy3(i, core).wait_send()
        copy3(i, 1 - core).wait_recv()
        at = pl.ds(pl.multiple_of(i * rows, rows), rows)
        for j in range(2):
            cols = slice(j * (model_dev // 2), (j + 1) * (model_dev // 2))
            update = jnp.dot(mixed[i], wout[layer, :, cols], preferred_element_type=F32)
            o_ref[at, cols] = (o_ref[at, cols].astype(F32) + update).astype(BF16)

    steps = layers * CHUNKS

    @pl.loop(0, steps + LAG)
    def _(k):
        pump(k, 0)

        @pl.when(k < steps)
        def _():
            project(k)

        pump(k, 1)

        @pl.when((k >= LAG - 1) & (k < steps + LAG - 1))
        def _():
            normalise(k - (LAG - 1))

        @pl.when(k >= LAG)
        def _():
            pool(k - LAG)

        @pl.when(k < steps)
        def _():
            join(k)

        @pl.when(k >= LAG)
        def _():
            finish(k - LAG)

    @pl.loop(0, layers)
    def _(layer):
        for side in range(2):
            for piece in range(2):
                for way in range(2):
                    @pl.loop(0, hops(way, piece))
                    def _(hop):
                        ring_copy(layer, side, piece, way, hop, False).wait_send()


def body(snake, sp, tp, stream, doc_ids, norm_gain, proj_in, mix_pool, pool_gain, proj_out):
    layers, model_dev, chan_dev = proj_in.shape
    tokens = stream.shape[0]
    rows = tokens // CHUNKS
    channels = chan_dev * sp
    half = channels // 2
    hops = sp // 2
    dma, vmem = pltpu.SemaphoreType.DMA, pltpu.VMEM
    return pl.pallas_call(
        functools.partial(mixer, sp, tp, snake),
        out_shape=jax.ShapeDtypeStruct(stream.shape, BF16),
        in_specs=[pl.BlockSpec(memory_space=pltpu.VMEM)] * 7,
        out_specs=pl.BlockSpec(memory_space=pltpu.VMEM),
        scratch_shapes=[
            vmem((layers, model_dev, channels), BF16),
            vmem((layers, channels, model_dev), BF16),
            vmem((CHUNKS, rows, half), BF16),
            vmem((CHUNKS, rows, half), BF16),
            vmem((CHUNKS, rows, half), BF16),
            vmem((CHUNKS, rows, half), BF16),
            vmem((2, CHUNKS, rows, half), BF16),
            vmem((CHUNKS, rows, channels), BF16),
            vmem((HALO + tokens, half), BF16),
            vmem((layers, HALO, half), BF16),
            vmem((CHUNKS, 8, rows), F32),
            vmem((CHUNKS, 8, rows), F32),
            vmem((CHUNKS, 8, rows), F32),
            vmem((2, CHUNKS, 8, rows), F32),
            vmem((2 * HALO + tokens, 128), F32),
            vmem((2 * HALO, 128), F32),
            vmem((HALO + tokens, 128), F32),
            vmem((layers, 1, model_dev), F32),
            vmem((layers, 1, half), F32),
            dma, dma,
            dma((layers, 2, 2, 2, hops)),
            dma((layers, 2, 2, 2, hops)),
            dma((2, CHUNKS)), dma((2, CHUNKS)),
            dma((2, CHUNKS)), dma((2, 2, CHUNKS)),
            dma((CHUNKS,)), dma((CHUNKS,)),
            dma((layers,)), dma((layers,)),
        ],
        compiler_params=pltpu.CompilerParams(
            collective_id=0, has_side_effects=True, vmem_limit_bytes=60 * 2**20),
    )(stream, doc_ids.reshape(-1, 128), norm_gain, proj_in, mix_pool, pool_gain, proj_out)


span_reach = 15


def shifted(value, axis, steps):
    count = lax.axis_size(axis)
    initial, last = (max(0, -steps), min(count, count - steps))
    return lax.ppermute(value, axis, [(source, source + steps) for source in range(initial, last)])


def span_pool(padded, labels, widths):
    kept = padded.shape[0] - span_reach
    own_label = labels[span_reach:]
    summed = jnp.zeros((kept, padded.shape[1]), jnp.float32)
    counted = jnp.zeros((kept, padded.shape[1]), jnp.float32)
    for offset in range(span_reach + 1):
        first = span_reach - offset
        member = (labels[first : first + kept] == own_label)[:, None] & (offset < widths)[None, :]
        factor = member.astype(jnp.float32)
        summed = summed + padded[first : first + kept] * factor
        counted = counted + factor
    return summed / counted - padded[span_reach:]


def plain_body(stream, doc_ids, norm_gain, proj_in, mix_pool, pool_gain, proj_out):
    width_dev = stream.shape[1]
    tp_count = lax.axis_size("tp")
    model_width = width_dev * tp_count
    group_size = mix_pool.shape[2]
    channels = proj_in.shape[2] * lax.axis_size("sp")
    local = channels // tp_count
    groups_dev = local // group_size
    column = lax.axis_index("tp")
    chan_ids = column * local + jnp.arange(local, dtype=jnp.int32)
    widths = jnp.left_shift(jnp.int32(2), chan_ids // group_size % 4)
    labels = (doc_ids + 1).astype(jnp.bfloat16)
    hidden_state = stream
    layer_count = proj_in.shape[0]
    in_whole, out_whole = (
        lax.all_gather(proj_in, "sp", axis=2, tiled=True),
        lax.all_gather(proj_out, "sp", axis=1, tiled=True),
    )
    for layer in range(layer_count):
        row_count = hidden_state.shape[0]
        wide = hidden_state.astype(jnp.float32)
        own_squares = jnp.sum(wide * wide, axis=1)
        gain = lax.dynamic_slice_in_dim(norm_gain[layer], column * width_dev, width_dev).astype(
            jnp.float32
        )
        gained = (wide * gain[None, :]).astype(jnp.bfloat16)
        partial_value = jnp.dot(gained, in_whole[layer], preferred_element_type=jnp.float32)
        squares = lax.psum(own_squares, "tp")
        summed_in = lax.psum_scatter(
            partial_value.astype(jnp.bfloat16), "tp", scatter_dimension=1, tiled=True
        ).astype(jnp.float32)
        row_scale = lax.rsqrt(squares / model_width + EPSILON)
        mixed_in = (summed_in * row_scale[:, None]).astype(jnp.bfloat16)
        before, before_labels = shifted((mixed_in[-span_reach:], labels[-span_reach:]), "sp", 1)
        padded = jnp.concatenate([before, mixed_in], axis=0).astype(jnp.float32)
        tags = jnp.concatenate([before_labels, labels], axis=0)
        pooled = span_pool(padded, tags, widths).astype(jnp.bfloat16)
        grouped = pooled.reshape(row_count, groups_dev, group_size)
        mixing = lax.dynamic_slice_in_dim(mix_pool[layer], column * groups_dev, groups_dev, 0)
        blended = jnp.einsum(
            "tgc,gcd->tgd", grouped, mixing, preferred_element_type=jnp.float32
        ).reshape(row_count, local)
        scale = lax.dynamic_slice_in_dim(pool_gain[layer], column * local, local).astype(
            jnp.float32
        )
        mixed = (blended * scale[None, :]).astype(jnp.bfloat16)
        full_mixed = lax.all_gather(mixed, "tp", axis=1, tiled=True)
        update = jnp.dot(full_mixed, out_whole[layer], preferred_element_type=jnp.float32)
        hidden_state = (wide + update).astype(jnp.bfloat16)
    return hidden_state


def solution(mesh):
    sp, tp = mesh.shape["sp"], mesh.shape["tp"]
    in_specs = (P("sp", "tp"), P("sp"), P(), P(None, "tp", "sp"), P(), P(), P(None, "sp", "tp"))

    def whole(stream, doc_ids, norm_gain, proj_in, mix_pool, pool_gain, proj_out):
        fits = tp == 4 and sp % 2 == 0 and proj_in.shape[2] // sp % 128 == 0 and mix_pool.shape[1] % 8 == 0
        part = functools.partial(body, True, sp, tp) if fits else plain_body
        return jax.shard_map(part, mesh=mesh, in_specs=in_specs, out_specs=P("sp", "tp"), check_vma=False)(
            stream, doc_ids, norm_gain, proj_in, mix_pool, pool_gain, proj_out)

    return whole
```

profile of v0, /device:TPU:0, one launch (start us, length us, event | category | flops | bytes accessed | tf_op | source)
XLA Modules:
  0.0 194.3 jit_solution(17263384590089187185)
XLA Ops:
  0.0 189.7 %shard_map.73 = bf16[2048,1024]{1,0:T(8,128)(2,1)} custom-call(bf16[2048,1024]{1,0:T(8,128)(2,1)} %x_ref.1, s32[16,128]{1,0:T(8,128)} %bitcast.1, bf16[3,4096]{1,0:T(4,128)(2,1)} %gains_ref.1, bf16[3,1024,128]{2,1,0:T(8,128)(2,1)} %win_ref.1, bf16[3,8,128,128]{3,2,1,0:T(8,128)(2,1)} %mix_ref.1, bf16[3,1024]{1,0:T(4,128)(2,1)} %pgains_ref.1, ...), custom_call_target="tpu_custom_call" | custom-call | tf_op jit(solution)/shard_map/pallas_call | solution.py:340
  189.7 4.6 %copy.9 = bf16[2048,1024]{1,0:T(8,128)(2,1)} copy(bf16[2048,1024]{1,0:T(8,128)(2,1)} %shard_map.73) | data formatting | bytes 8388608
where the time goes:
time: 194 us
  Pallas kernels  190 us (98%)
  local copies, waits for them, and re-layouts  4.64 us (2%)
    pallas_call x1, Pallas kernels, body(): pl.pallas_call(functools.partial(mixer, sp, tp, snake), out_shape=jax.Sha...  190 us
    unnamed x1, local copies, waits for them, and re-layouts  4.64 us

commit v1 on v0

v1 whole, which is shorter than its diff:
```python
import functools

import jax
import jax.numpy as jnp
from jax import lax
from jax.experimental import pallas as pl
from jax.experimental.pallas import tpu as pltpu
from jax.sharding import PartitionSpec as P

EPSILON = 1e-06
HALO = 16
CHUNKS = 8
EDGE = 3
RING = 8
LAYERS = 3
MESH = pl.DeviceIdType.MESH
F32, BF16 = jnp.float32, jnp.bfloat16


def mixer(sp, tp, x_hbm, doc_ref, gains_ref, win_hbm, mix_ref, pgains_ref, wout_hbm, o_hbm,
          h, win, wout, gbuf, send1, own1, recv1, sum2, recv2, mixed, zbuf, hrecv,
          sq_own, sq_in, scale_ref, labels, before_labels, pos_ref, gain_ref, pgain_ref,
          xs, ws, os, ls, lr, ring_s, ring_r, sqs, sqr, s1, r1, s2, r2, s3, r3, hs, hr):
    layers, model_dev, chan_dev = win_hbm.shape
    tokens = h.shape[0]
    rows = tokens // CHUNKS
    channels = chan_dev * sp
    half = channels // 2
    group = mix_ref.shape[-1]
    own_groups = half // group
    model = model_dev * tp
    row_dev = wout_hbm.shape[1]
    last = CHUNKS - 1
    s, t = lax.axis_index("sp"), lax.axis_index("tp")
    core = lax.rem(t, 2)
    partner = t + 1 - 2 * core
    across = lax.rem(t + 2, tp)
    diagonal = lax.rem(partner + 2, tp)

    def place(device):
        z, y = device // 2, lax.rem(device, 2)
        return z * (1 - y) + (sp - 1 - z) * y

    def device_at(place):
        up = place // (sp // 2)
        return 2 * (place * (1 - up) + (sp - 1 - place) * up) + up

    here = place(s)
    after, before = device_at(lax.rem(here + 1, sp)), device_at(lax.rem(here + sp - 1, sp))
    following, leading = lax.rem(s + 1, sp), lax.rem(s + sp - 1, sp)

    def columns(device):
        return pl.ds(pl.multiple_of(device * chan_dev, chan_dev), chan_dev)

    def ring_view(layer, side, piece, source):
        if side == 0:
            part = model_dev // 2
            return win.at[layer, pl.ds(pl.multiple_of(piece * part, part), part), columns(source)]
        part = row_dev // 2
        return wout.at[layer, pl.ds(pl.multiple_of(source * row_dev + piece * part, part), part)]

    def ring_copy(layer, side, way, turn, back):
        hop = turn // 2 + back
        piece = lax.rem(turn + way, 2)
        origin = here - hop + sp if way == 0 else here + hop
        view = ring_view(layer, side, piece, device_at(lax.rem(origin, sp)))
        return pltpu.make_async_remote_copy(
            src_ref=view, dst_ref=view,
            send_sem=ring_s.at[layer, side, way, turn], recv_sem=ring_r.at[layer, side, way, turn],
            device_id={"sp": after if way == 0 else before}, device_id_type=MESH)

    turns = sp - 1
    items = 2 * layers

    def arrive(index):
        item, turn = index // turns, lax.rem(index, turns)
        layer, side = item // 2, lax.rem(item, 2)
        for which in range(2):
            @pl.when(side == which)
            def _():
                for way in range(2):
                    ring_copy(layer, which, way, turn, 1).wait_recv()

                @pl.when(turn < turns - 2)
                def _():
                    for way in range(2):
                        ring_copy(layer, which, way, turn + 2, 0).start()

                @pl.when((turn >= turns - 3) & (turn < turns - 1) & (item + 1 < items))
                def _():
                    for way in range(2):
                        ring_copy(layer + which, 1 - which, way, turn - (turns - 3), 0).start()

    def at(i):
        return pl.ds(pl.multiple_of(i * rows, rows), rows)

    def load_x(i):
        return pltpu.make_async_copy(x_hbm.at[at(i)], h.at[at(i)], xs.at[i])

    def load_w(layer, side):
        if side == 0:
            return pltpu.make_async_copy(win_hbm.at[layer], win.at[layer, :, columns(s)], ws.at[layer, side])
        return pltpu.make_async_copy(
            wout_hbm.at[layer], wout.at[layer, pl.ds(pl.multiple_of(s * row_dev, row_dev), row_dev)], ws.at[layer, side])

    def store_out(i):
        return pltpu.make_async_copy(h.at[at(i)], o_hbm.at[at(i)], os.at[i])

    load_w(0, 0).start()
    for i in range(CHUNKS):
        load_x(last - i).start()
    for layer in range(layers):
        for side in range(2):
            if layer + side > 0:
                load_w(layer, side).start()

    barrier = pltpu.get_barrier_semaphore()
    peers = ({"tp": partner}, {"tp": across}, {"tp": diagonal},
             {"sp": after}, {"sp": before}, {"sp": following}, {"sp": leading})
    for peer in peers:
        pl.semaphore_signal(barrier, inc=1, device_id=peer, device_id_type=MESH)
    own_gain = gains_ref[:, pl.ds(pl.multiple_of(t * model_dev, model_dev), model_dev)].astype(F32)
    own_pgain = pgains_ref[:, pl.ds(pl.multiple_of(core * half, half), half)].astype(F32)
    for layer in range(layers):
        gain_ref[layer] = own_gain[layer:layer + 1]
        pgain_ref[layer] = own_pgain[layer:layer + 1]
    reach = 2 * HALO
    documents = doc_ref[...].astype(F32)
    for j in range(tokens // 128):
        labels[pl.ds(reach + j * 128, 128)] = jnp.broadcast_to(documents[j:j + 1], (128, 128)).T
    load_w(0, 0).wait()
    pl.semaphore_wait(barrier, len(peers))
    for turn in range(2):
        for way in range(2):
            ring_copy(0, 0, way, turn, 0).start()
    label_copy = pltpu.make_async_remote_copy(
        src_ref=labels.at[pl.ds(tokens, reach)], dst_ref=before_labels, send_sem=ls, recv_sem=lr,
        device_id={"sp": following}, device_id_type=MESH)
    label_copy.start()
    for i in range(CHUNKS):
        load_x(last - i).wait()
    for layer in range(layers):
        for side in range(2):
            if layer + side > 0:
                load_w(layer, side).wait()

    def distances(ext):
        run = (pltpu.roll(ext, 1, 0) == ext).astype(F32)
        size = 1
        while size < HALO:
            run = run + jnp.where(run == float(size), pltpu.roll(run, size, 0), 0.0)
            size *= 2
        return run[HALO:]

    def prepare():
        label_copy.wait()
        labels[pl.ds(0, reach)] = jnp.where(s == 0, -1.0, before_labels[...])
        pos_ref[pl.ds(0, HALO)] = distances(labels[pl.ds(0, reach)])

        @pl.loop(0, CHUNKS)
        def _(i):
            pos_ref[pl.ds(pl.multiple_of(HALO + i * rows, HALO), rows)] = distances(
                labels[pl.ds(pl.multiple_of(HALO + i * rows, HALO), rows + HALO)])

    def copy_sq(layer, i):
        par = lax.rem(layer, 2)
        return [pltpu.make_async_remote_copy(
            src_ref=sq_own.at[i], dst_ref=sq_in.at[j, par, i], send_sem=sqs.at[j, i], recv_sem=sqr.at[j, par, i],
            device_id={"tp": peer}, device_id_type=MESH)
            for j, peer in enumerate((partner, across, diagonal))]

    def copy1(i, lg):
        return pltpu.make_async_remote_copy(
            src_ref=send1.at[lg, i], dst_ref=recv1.at[lg, i], send_sem=s1.at[lg, i], recv_sem=r1.at[lg, i],
            device_id={"tp": partner}, device_id_type=MESH)

    def copy2(layer, i, lg):
        par = lax.rem(layer, 2)
        return pltpu.make_async_remote_copy(
            src_ref=sum2.at[lg, i], dst_ref=recv2.at[par, lg, i], send_sem=s2.at[lg, i], recv_sem=r2.at[par, lg, i],
            device_id={"tp": across}, device_id_type=MESH)

    def copy3(i, side, lg):
        view = mixed.at[i, :, pl.ds(pl.multiple_of(side * half + lg * group, group), group)]
        return pltpu.make_async_remote_copy(
            src_ref=view, dst_ref=view, send_sem=s3.at[lg, i], recv_sem=r3.at[lg, i],
            device_id={"tp": partner}, device_id_type=MESH)

    def halo_copy(layer, lg):
        return pltpu.make_async_remote_copy(
            src_ref=zbuf.at[lg, pl.ds(tokens, HALO)], dst_ref=hrecv.at[layer, lg],
            send_sem=hs.at[layer, lg], recv_sem=hr.at[layer, lg],
            device_id={"sp": following}, device_id_type=MESH)

    def groups_of(distance):
        return (device_at(lax.rem(here - distance + sp, sp)), device_at(lax.rem(here + distance, sp)))

    def owned(g):
        return g // own_groups == core

    def local(g):
        return lax.rem(g, own_groups)

    def gained_of(layer, i):
        wide = h[at(i)].astype(F32)
        squares = wide * wide
        lanes = squares[:, :128]
        for j in range(1, model_dev // 128):
            lanes = lanes + squares[:, j * 128:(j + 1) * 128]
        sq_own[i] = jnp.sum(lanes.T, axis=0, keepdims=True)
        gained = (wide * gain_ref[layer]).astype(BF16)
        for c in copy_sq(layer, i):
            c.start()
        return gained

    def deliver(i, g, value):
        @pl.when(owned(g))
        def _():
            own1[local(g), i] = value

        @pl.when(jnp.logical_not(owned(g)))
        def _():
            send1[local(g), i] = value
            copy1(i, local(g)).start()

    def project_groups(layer, distance, i):
        low, high = groups_of(distance)

        @pl.when(lax.rem(distance, sp // 2) == 0)
        def _():
            part = jnp.dot(gbuf[i], win[layer, :, columns(low)], preferred_element_type=F32).astype(BF16)
            deliver(i, low, part)

        @pl.when(lax.rem(distance, sp // 2) > 0)
        def _():
            weights = jnp.concatenate([win[layer, :, columns(low)], win[layer, :, columns(high)]], axis=1)
            part = jnp.dot(gbuf[i], weights, preferred_element_type=F32).astype(BF16)
            deliver(i, low, part[:, :group])
            deliver(i, high, part[:, group:])

    def project(layer, i):
        gained = gained_of(layer, i)
        other = pl.ds(pl.multiple_of((1 - core) * half, half), half)
        part = jnp.dot(gained, win[layer, :, other], preferred_element_type=F32).astype(BF16)
        for lg in range(own_groups):
            send1[lg, i] = part[:, lg * group:(lg + 1) * group]
            copy1(i, lg).start()
        mine = pl.ds(pl.multiple_of(core * half, half), half)
        part = jnp.dot(gained, win[layer, :, mine], preferred_element_type=F32).astype(BF16)
        for lg in range(own_groups):
            own1[lg, i] = part[:, lg * group:(lg + 1) * group]

    def add_up(layer, i, lg):
        sum2[lg, i] = (own1[lg, i].astype(F32) + recv1[lg, i].astype(F32)).astype(BF16)
        copy2(layer, i, lg).start()

    def each_group(distance, act):
        low, high = groups_of(distance)
        act(low)

        @pl.when(lax.rem(distance, sp // 2) > 0)
        def _():
            act(high)

    def join_groups(layer, distance, i):
        def act(g):
            @pl.when(owned(g))
            def _():
                copy1(i, local(g)).wait_recv()
                add_up(layer, i, local(g))

            @pl.when(jnp.logical_not(owned(g)))
            def _():
                copy1(i, local(g)).wait_send()
        each_group(distance, act)

    def join(layer, i):
        for lg in range(own_groups):
            copy1(i, lg).wait()
            add_up(layer, i, lg)

    def rescale(layer, i):
        par = lax.rem(layer, 2)
        total = sq_own[i]
        for j, c in enumerate(copy_sq(layer, i)):
            c.wait()
            total = total + sq_in[j, par, i]
        scale_ref[i] = jnp.broadcast_to(lax.rsqrt(total / model + EPSILON), (128, rows)).T

    def normalise(layer, i, lg):
        par = lax.rem(layer, 2)
        copy2(layer, i, lg).wait()
        summed = sum2[lg, i].astype(F32) + recv2[par, lg, i].astype(F32)
        zbuf[lg, pl.ds(pl.multiple_of(HALO + i * rows, HALO), rows)] = (summed * scale_ref[i]).astype(BF16)

        @pl.when(i == last)
        def _():
            halo_copy(layer, lg).start()

    def pool(layer, i, lg):
        @pl.when(i == 0)
        def _():
            halo_copy(layer, lg).wait()
            zbuf[lg, pl.ds(0, HALO)] = hrecv[layer, lg]

        wide_at = pl.ds(pl.multiple_of(i * rows, HALO), rows + HALO)
        pos = pos_ref[wide_at]
        z = zbuf[lg, wide_at].astype(F32)
        window = 2 ** (1 + lg % 4)
        total = z
        size = 1
        while size < window:
            total = total + jnp.where(pos >= size, pltpu.roll(total, size, 0), 0.0)
            size *= 2
        count = jnp.minimum(pos[HALO:] + 1.0, float(window))
        pooled = (total[HALO:] / count - z[HALO:]).astype(BF16)
        blended = jnp.dot(pooled, mix_ref[layer, core * own_groups + lg], preferred_element_type=F32)
        place_at = pl.ds(pl.multiple_of(core * half + lg * group, group), group)
        mixed[i, :, place_at] = (blended * pgain_ref[layer, :, lg * group:(lg + 1) * group]).astype(BF16)
        copy3(i, core, lg).start()

    def finish(layer, i):
        for lg in range(own_groups):
            copy3(i, core, lg).wait_send()
            copy3(i, 1 - core, lg).wait_recv()
        for j in range(2):
            cols = slice(j * (model_dev // 2), (j + 1) * (model_dev // 2))
            update = jnp.dot(mixed[i], wout[layer, :, cols], preferred_element_type=F32)
            h[at(i), cols] = (h[at(i), cols].astype(F32) + update).astype(BF16)

        @pl.when(layer == layers - 1)
        def _():
            store_out(i).start()

    spans = sp // 2 + 1

    @pl.loop(0, layers + 1)
    def _(layer):
        edge = EDGE + layer
        ending = layer // layers
        live = layer < layers
        slots = (spans + edge) * (1 - ending) + 2 * ending
        done = layer - 1

        @pl.loop(0, slots)
        def _(q):
            turn = 2 * (q - 1 + (sp - 1) * layer + 2 * (layer // 2))
            pumping = live & (turn < turns * items) & ((q > 0) | (layer > 1))
            early = (q > 0) & (q < spans - 1)

            @pl.when(pumping)
            def _():
                arrive(turn)

            @pl.when(pumping & early)
            def _():
                arrive(turn + 1)

            @pl.when(live & (q == 0))
            def _():
                @pl.loop(0, CHUNKS - edge)
                def _(j):
                    gbuf[last - j] = gained_of(layer, last - j)

            @pl.when(live & (q < spans))
            def _():
                @pl.loop(0, CHUNKS - edge)
                def _(j):
                    project_groups(layer, q, last - j)

            @pl.when(q >= spans)
            def _():
                project(layer, edge - 1 - (q - spans))

            @pl.when((layer == 0) & (q == 1))
            def _():
                prepare()

            @pl.when(live & (q > 1) & (q < spans + 2))
            def _():
                distance = q - 2

                @pl.loop(0, CHUNKS - edge)
                def _(j):
                    @pl.when(distance == 0)
                    def _():
                        rescale(layer, last - j)

                    def act(g):
                        @pl.when(owned(g))
                        def _():
                            normalise(layer, last - j, local(g))
                    each_group(distance, act)

                @pl.loop(0, CHUNKS - edge - 1)
                def _(j):
                    def act(g):
                        for lg in range(own_groups):
                            @pl.when(owned(g) & (local(g) == lg))
                            def _():
                                pool(layer, last - j, lg)
                    each_group(distance, act)

            old = (q < 2) & (layer > 0)

            @pl.when(old | (q >= spans + 2))
            def _():
                fresh = q // (spans + 2)
                of = layer - 1 + fresh
                i = (1 - q) * (1 - fresh) + (edge - 1 - (q - 2 - spans)) * fresh
                rescale(of, i)
                for lg in range(own_groups):
                    normalise(of, i, lg)

                @pl.loop(0, 1 + (1 - fresh) * q)
                def _(j):
                    for lg in range(own_groups):
                        pool(of, i + 1 - j, lg)

            @pl.when(pumping & jnp.logical_not(early))
            def _():
                arrive(turn + 1)

            @pl.when(live & (q < spans))
            def _():
                @pl.loop(0, CHUNKS - edge)
                def _(j):
                    join_groups(layer, q, last - j)

            @pl.when(q >= spans)
            def _():
                join(layer, edge - 1 - (q - spans))

            @pl.when((q == spans + 2) & live)
            def _():
                @pl.loop(0, CHUNKS - edge - 1)
                def _(j):
                    finish(layer, last - j)

            one = (q < 4) & (layer > 0)

            @pl.when(one | (q > spans + 2))
            def _():
                fresh = q // (spans + 3)
                first = (3 - q - q * ending) * (1 - fresh) + (edge - (q - spans - 3)) * fresh

                @pl.loop(0, 1 + ending)
                def _(j):
                    finish(layer - 1 + fresh, first - j)

    @pl.loop(0, layers)
    def _(layer):
        for side in range(2):
            for way in range(2):
                @pl.loop(0, turns)
                def _(turn):
                    ring_copy(layer, side, way, turn, 0).wait_send()

    @pl.loop(0, CHUNKS)
    def _(i):
        store_out(i).wait()


def body(sp, tp, stream, doc_ids, norm_gain, proj_in, mix_pool, pool_gain, proj_out):
    layers, model_dev, chan_dev = proj_in.shape
    tokens = stream.shape[0]
    rows = tokens // CHUNKS
    channels = chan_dev * sp
    half = channels // 2
    group = mix_pool.shape[-1]
    own = half // group
    dma, vmem = pltpu.SemaphoreType.DMA, pltpu.VMEM
    local, remote = pl.BlockSpec(memory_space=pltpu.VMEM), pl.BlockSpec(memory_space=pl.ANY)
    return pl.pallas_call(
        functools.partial(mixer, sp, tp),
        out_shape=jax.ShapeDtypeStruct(stream.shape, BF16),
        in_specs=[remote, local, local, remote, local, local, remote],
        out_specs=remote,
        scratch_shapes=[
            vmem((tokens, model_dev), BF16),
            vmem((layers, model_dev, channels), BF16),
            vmem((layers, channels, model_dev), BF16),
            vmem((CHUNKS, rows, model_dev), BF16),
            vmem((own, CHUNKS, rows, group), BF16),
            vmem((own, CHUNKS, rows, group), BF16),
            vmem((own, CHUNKS, rows, group), BF16),
            vmem((own, CHUNKS, rows, group), BF16),
            vmem((2, own, CHUNKS, rows, group), BF16),
            vmem((CHUNKS, rows, channels), BF16),
            vmem((own, HALO + tokens, group), BF16),
            vmem((layers, own, HALO, group), BF16),
            vmem((CHUNKS, 1, rows), F32),
            vmem((3, 2, CHUNKS, 1, rows), F32),
            vmem((CHUNKS, rows, 128), F32),
            vmem((2 * HALO + tokens, 128), F32),
            vmem((2 * HALO, 128), F32),
            vmem((HALO + tokens, 128), F32),
            vmem((layers, 1, model_dev), F32),
            vmem((layers, 1, half), F32),
            dma((CHUNKS,)), dma((layers, 2)), dma((CHUNKS,)),
            dma, dma,
            dma((layers, 2, 2, sp - 1)), dma((layers, 2, 2, sp - 1)),
            dma((3, CHUNKS)), dma((3, 2, CHUNKS)),
            dma((own, CHUNKS)), dma((own, CHUNKS)),
            dma((own, CHUNKS)), dma((2, own, CHUNKS)),
            dma((own, CHUNKS)), dma((own, CHUNKS)),
            dma((layers, own)), dma((layers, own)),
        ],
        compiler_params=pltpu.CompilerParams(
            collective_id=0, has_side_effects=True, vmem_limit_bytes=60 * 2**20),
    )(stream, doc_ids.reshape(-1, 128), norm_gain, proj_in, mix_pool, pool_gain, proj_out)


span_reach = 15


def shifted(value, axis, steps):
    count = lax.axis_size(axis)
    initial, last = (max(0, -steps), min(count, count - steps))
    return lax.ppermute(value, axis, [(source, source + steps) for source in range(initial, last)])


def span_pool(padded, labels, widths):
    kept = padded.shape[0] - span_reach
    own_label = labels[span_reach:]
    summed = jnp.zeros((kept, padded.shape[1]), jnp.float32)
    counted = jnp.zeros((kept, padded.shape[1]), jnp.float32)
    for offset in range(span_reach + 1):
        first = span_reach - offset
        member = (labels[first : first + kept] == own_label)[:, None] & (offset < widths)[None, :]
        factor = member.astype(jnp.float32)
        summed = summed + padded[first : first + kept] * factor
        counted = counted + factor
    return summed / counted - padded[span_reach:]


def plain_body(stream, doc_ids, norm_gain, proj_in, mix_pool, pool_gain, proj_out):
    width_dev = stream.shape[1]
    tp_count = lax.axis_size("tp")
    model_width = width_dev * tp_count
    group_size = mix_pool.shape[2]
    channels = proj_in.shape[2] * lax.axis_size("sp")
    local = channels // tp_count
    groups_dev = local // group_size
    column = lax.axis_index("tp")
    chan_ids = column * local + jnp.arange(local, dtype=jnp.int32)
    widths = jnp.left_shift(jnp.int32(2), chan_ids // group_size % 4)
    labels = (doc_ids + 1).astype(jnp.bfloat16)
    hidden_state = stream
    layer_count = proj_in.shape[0]
    in_whole, out_whole = (
        lax.all_gather(proj_in, "sp", axis=2, tiled=True),
        lax.all_gather(proj_out, "sp", axis=1, tiled=True),
    )
    for layer in range(layer_count):
        row_count = hidden_state.shape[0]
        wide = hidden_state.astype(jnp.float32)
        own_squares = jnp.sum(wide * wide, axis=1)
        gain = lax.dynamic_slice_in_dim(norm_gain[layer], column * width_dev, width_dev).astype(
            jnp.float32
        )
        gained = (wide * gain[None, :]).astype(jnp.bfloat16)
        partial_value = jnp.dot(gained, in_whole[layer], preferred_element_type=jnp.float32)
        squares = lax.psum(own_squares, "tp")
        summed_in = lax.psum_scatter(
            partial_value.astype(jnp.bfloat16), "tp", scatter_dimension=1, tiled=True
        ).astype(jnp.float32)
        row_scale = lax.rsqrt(squares / model_width + EPSILON)
        mixed_in = (summed_in * row_scale[:, None]).astype(jnp.bfloat16)
        before, before_labels = shifted((mixed_in[-span_reach:], labels[-span_reach:]), "sp", 1)
        padded = jnp.concatenate([before, mixed_in], axis=0).astype(jnp.float32)
        tags = jnp.concatenate([before_labels, labels], axis=0)
        pooled = span_pool(padded, tags, widths).astype(jnp.bfloat16)
        grouped = pooled.reshape(row_count, groups_dev, group_size)
        mixing = lax.dynamic_slice_in_dim(mix_pool[layer], column * groups_dev, groups_dev, 0)
        blended = jnp.einsum(
            "tgc,gcd->tgd", grouped, mixing, preferred_element_type=jnp.float32
        ).reshape(row_count, local)
        scale = lax.dynamic_slice_in_dim(pool_gain[layer], column * local, local).astype(
            jnp.float32
        )
        mixed = (blended * scale[None, :]).astype(jnp.bfloat16)
        full_mixed = lax.all_gather(mixed, "tp", axis=1, tiled=True)
        update = jnp.dot(full_mixed, out_whole[layer], preferred_element_type=jnp.float32)
        hidden_state = (wide + update).astype(jnp.bfloat16)
    return hidden_state


def solution(mesh):
    sp, tp = mesh.shape["sp"], mesh.shape["tp"]
    in_specs = (P("sp", "tp"), P("sp"), P(), P(None, "tp", "sp"), P(), P(), P(None, "sp", "tp"))

    def whole(stream, doc_ids, norm_gain, proj_in, mix_pool, pool_gain, proj_out):
        layers, _, channels = proj_in.shape
        group = mix_pool.shape[2]
        fits = (tp == 4 and sp == RING and layers == LAYERS and channels == sp * group and group == 128
                and mix_pool.shape[1] % 8 == 0 and stream.shape[0] % (sp * CHUNKS * 128) == 0)
        part = functools.partial(body, sp, tp) if fits else plain_body
        return jax.shard_map(part, mesh=mesh, in_specs=in_specs, out_specs=P("sp", "tp"), check_vma=False)(
            stream, doc_ids, norm_gain, proj_in, mix_pool, pool_gain, proj_out)

    return whole
```

time: 194 us -> 181 us (0.933)
  Pallas kernels: 190 us -> 177 us
    pallas_call x1, Pallas kernels: 190 us -> 177 us  [body(): pl.pallas_call(functools.partial(mixer, sp, tp), out_shape=jax.ShapeDtype...]
where the time goes in v1:
time: 181 us
  Pallas kernels  177 us (98%)
  local copies, waits for them, and re-layouts  4.64 us (3%)
    pallas_call x1, Pallas kernels, body(): pl.pallas_call(functools.partial(mixer, sp, tp), out_shape=jax.ShapeDtype...  177 us
    unnamed x1, local copies, waits for them, and re-layouts  4.64 us

profile of v1, /device:TPU:0, one launch (start us, length us, event | category | flops | bytes accessed | tf_op | source)
XLA Modules:
  0.0 181.2 jit_solution(15615323199657313770)
XLA Ops:
  0.0 176.5 %shard_map.73 = bf16[2048,1024]{1,0:T(8,128)(2,1)} custom-call(bf16[2048,1024]{1,0:T(8,128)(2,1)} %x_hbm.1, s32[16,128]{1,0:T(8,128)} %bitcast.1, bf16[3,4096]{1,0:T(4,128)(2,1)} %gains_ref.1, bf16[3,1024,128]{2,1,0:T(8,128)(2,1)} %win_hbm.1, bf16[3,8,128,128]{3,2,1,0:T(8,128)(2,1)} %mix_ref.1, bf16[3,1024]{1,0:T(4,128)(2,1)} %pgains_ref.1, ...), custom_call_target="tpu_custom_call" | custom-call | tf_op jit(solution)/shard_map/pallas_call | solution.py:474
  176.5 4.6 %copy.9 = bf16[2048,1024]{1,0:T(8,128)(2,1)} copy(bf16[2048,1024]{1,0:T(8,128)(2,1)} %shard_map.73) | data formatting | bytes 8388608

commit v2 on v1

--- a/solution.py
+++ b/solution.py
@@ -17,10 +17,10 @@
 F32, BF16 = jnp.float32, jnp.bfloat16
 
 
-def mixer(sp, tp, x_hbm, doc_ref, gains_ref, win_hbm, mix_ref, pgains_ref, wout_hbm, o_hbm,
-          h, win, wout, gbuf, send1, own1, recv1, sum2, recv2, mixed, zbuf, hrecv,
+def mixer(sp, tp, x_hbm, doc_ref, gains_ref, win_hbm, mix_ref, pgains_ref, wout_hbm, h,
+          win, wout, gbuf, send1, own1, recv1, sum2, recv2, mixed, zbuf, hrecv,
           sq_own, sq_in, scale_ref, labels, before_labels, pos_ref, gain_ref, pgain_ref,
-          xs, ws, os, ls, lr, ring_s, ring_r, sqs, sqr, s1, r1, s2, r2, s3, r3, hs, hr):
+          xs, ws, ls, lr, ring_s, ring_r, sqs, sqr, s1, r1, s2, r2, s3, r3, hs, hr):
     layers, model_dev, chan_dev = win_hbm.shape
     tokens = h.shape[0]
     rows = tokens // CHUNKS
@@ -103,9 +103,6 @@
         return pltpu.make_async_copy(
             wout_hbm.at[layer], wout.at[layer, pl.ds(pl.multiple_of(s * row_dev, row_dev), row_dev)], ws.at[layer, side])
 
-    def store_out(i):
-        return pltpu.make_async_copy(h.at[at(i)], o_hbm.at[at(i)], os.at[i])
-
     load_w(0, 0).start()
     for i in range(CHUNKS):
         load_x(last - i).start()
@@ -124,25 +121,15 @@
     for layer in range(layers):
         gain_ref[layer] = own_gain[layer:layer + 1]
         pgain_ref[layer] = own_pgain[layer:layer + 1]
-    reach = 2 * HALO
-    documents = doc_ref[...].astype(F32)
-    for j in range(tokens // 128):
-        labels[pl.ds(reach + j * 128, 128)] = jnp.broadcast_to(documents[j:j + 1], (128, 128)).T
     load_w(0, 0).wait()
     pl.semaphore_wait(barrier, len(peers))
     for turn in range(2):
         for way in range(2):
             ring_copy(0, 0, way, turn, 0).start()
+    reach = 2 * HALO
     label_copy = pltpu.make_async_remote_copy(
         src_ref=labels.at[pl.ds(tokens, reach)], dst_ref=before_labels, send_sem=ls, recv_sem=lr,
         device_id={"sp": following}, device_id_type=MESH)
-    label_copy.start()
-    for i in range(CHUNKS):
-        load_x(last - i).wait()
-    for layer in range(layers):
-        for side in range(2):
-            if layer + side > 0:
-                load_w(layer, side).wait()
 
     def distances(ext):
         run = (pltpu.roll(ext, 1, 0) == ext).astype(F32)
@@ -153,6 +140,18 @@
         return run[HALO:]
 
     def prepare():
+        for i in range(EDGE):
+            load_x(i).wait()
+        for layer in range(layers):
+            for side in range(2):
+                if layer + side > 0:
+                    load_w(layer, side).wait()
+        documents = doc_ref[...].astype(F32)
+        for j in range(tokens // 128):
+            labels[pl.ds(reach + j * 128, 128)] = jnp.broadcast_to(documents[j:j + 1], (128, 128)).T
+        label_copy.start()
+
+    def measure():
         label_copy.wait()
         labels[pl.ds(0, reach)] = jnp.where(s == 0, -1.0, before_labels[...])
         pos_ref[pl.ds(0, HALO)] = distances(labels[pl.ds(0, reach)])
@@ -328,9 +327,6 @@
             update = jnp.dot(mixed[i], wout[layer, :, cols], preferred_element_type=F32)
             h[at(i), cols] = (h[at(i), cols].astype(F32) + update).astype(BF16)
 
-        @pl.when(layer == layers - 1)
-        def _():
-            store_out(i).start()
 
     spans = sp // 2 + 1
 
@@ -340,41 +336,75 @@
         ending = layer // layers
         live = layer < layers
         slots = (spans + edge) * (1 - ending) + 2 * ending
-        done = layer - 1
 
         @pl.loop(0, slots)
         def _(q):
-            turn = 2 * (q - 1 + (sp - 1) * layer + 2 * (layer // 2))
-            pumping = live & (turn < turns * items) & ((q > 0) | (layer > 1))
-            early = (q > 0) & (q < spans - 1)
-
-            @pl.when(pumping)
+            later = layer - layer // 2
+            turn = 2 * q - q // spans + later * (15 - (q + 9) // 10) + (layer // 2) * 16
+            single = (q == spans - 1) | ((q == 0) & (layer > 0))
+            count = CHUNKS - edge
+
+            @pl.when(live & (q < spans))
+            def _():
+                @pl.loop(0, count)
+                def _(j):
+                    @pl.when(q == 0)
+                    def _():
+                        @pl.when(layer == 0)
+                        def _():
+                            load_x(last - j).wait()
+
+                        gbuf[last - j] = gained_of(layer, last - j)
+
+                    project_groups(layer, q, last - j)
+
+                    @pl.when(j >= 2)
+                    def _():
+                        join_groups(layer, q, last - j + 2)
+
+            @pl.when(q >= spans)
+            def _():
+                project(layer, edge - 1 - (q - spans))
+
+            one = (q < 4) & (layer > 0)
+
+            @pl.when(one | (q > spans + 2))
+            def _():
+                fresh = q // (spans + 3)
+                finish(layer - 1 + fresh, (3 - q) * (1 - fresh) + (edge - (q - spans - 3)) * fresh)
+
+            @pl.when(live & (q < spans))
+            def _():
+                for j in range(2):
+                    join_groups(layer, q, edge + 1 - j)
+
+            @pl.when(q >= spans)
+            def _():
+                join(layer, edge - 1 - (q - spans))
+
+            @pl.when(live & (turn < turns * items))
             def _():
                 arrive(turn)
 
-            @pl.when(pumping & early)
+            @pl.when((q == spans + 2) & live)
+            def _():
+                @pl.loop(0, CHUNKS - edge - 1)
+                def _(j):
+                    finish(layer, last - j)
+
+            second = live & (turn + 1 < turns * items) & jnp.logical_not(single)
+
+            @pl.when(second & (q == spans + 2))
             def _():
                 arrive(turn + 1)
 
-            @pl.when(live & (q == 0))
-            def _():
-                @pl.loop(0, CHUNKS - edge)
-                def _(j):
-                    gbuf[last - j] = gained_of(layer, last - j)
-
-            @pl.when(live & (q < spans))
-            def _():
-                @pl.loop(0, CHUNKS - edge)
-                def _(j):
-                    project_groups(layer, q, last - j)
-
-            @pl.when(q >= spans)
-            def _():
-                project(layer, edge - 1 - (q - spans))
+            @pl.when((layer == 0) & (q == 0))
+            def _():
+                prepare()
 
             @pl.when((layer == 0) & (q == 1))
             def _():
-                prepare()
+                measure()
 
             @pl.when(live & (q > 1) & (q < spans + 2))
             def _():
@@ -417,36 +447,12 @@
                     for lg in range(own_groups):
                         pool(of, i + 1 - j, lg)
 
-            @pl.when(pumping & jnp.logical_not(early))
+            @pl.when(second & (q != spans + 2))
             def _():
                 arrive(turn + 1)
 
-            @pl.when(live & (q < spans))
-            def _():
-                @pl.loop(0, CHUNKS - edge)
-                def _(j):
-                    join_groups(layer, q, last - j)
-
-            @pl.when(q >= spans)
-            def _():
-                join(layer, edge - 1 - (q - spans))
-
-            @pl.when((q == spans + 2) & live)
-            def _():
-                @pl.loop(0, CHUNKS - edge - 1)
-                def _(j):
-                    finish(layer, last - j)
-
-            one = (q < 4) & (layer > 0)
-
-            @pl.when(one | (q > spans + 2))
-            def _():
-                fresh = q // (spans + 3)
-                first = (3 - q - q * ending) * (1 - fresh) + (edge - (q - spans - 3)) * fresh
-
-                @pl.loop(0, 1 + ending)
-                def _(j):
-                    finish(layer - 1 + fresh, first - j)
+    for i in range(2):
+        finish(layers - 1, 1 - i)
 
     @pl.loop(0, layers)
     def _(layer):
@@ -455,10 +461,6 @@
                 @pl.loop(0, turns)
                 def _(turn):
                     ring_copy(layer, side, way, turn, 0).wait_send()
-
-    @pl.loop(0, CHUNKS)
-    def _(i):
-        store_out(i).wait()
 
 
 def body(sp, tp, stream, doc_ids, norm_gain, proj_in, mix_pool, pool_gain, proj_out):
@@ -473,11 +475,10 @@
     local, remote = pl.BlockSpec(memory_space=pltpu.VMEM), pl.BlockSpec(memory_space=pl.ANY)
     return pl.pallas_call(
         functools.partial(mixer, sp, tp),
-        out_shape=jax.ShapeDtypeStruct(stream.shape, BF16),
+        out_shape=pltpu.VMEM(stream.shape, BF16),
         in_specs=[remote, local, local, remote, local, local, remote],
-        out_specs=remote,
+        out_specs=local,
         scratch_shapes=[
-            vmem((tokens, model_dev), BF16),
             vmem((layers, model_dev, channels), BF16),
             vmem((layers, channels, model_dev), BF16),
             vmem((CHUNKS, rows, model_dev), BF16),
@@ -497,7 +498,7 @@
             vmem((HALO + tokens, 128), F32),
             vmem((layers, 1, model_dev), F32),
             vmem((layers, 1, half), F32),
-            dma((CHUNKS,)), dma((layers, 2)), dma((CHUNKS,)),
+            dma((CHUNKS,)), dma((layers, 2)),
             dma, dma,
             dma((layers, 2, 2, sp - 1)), dma((layers, 2, 2, sp - 1)),
             dma((3, CHUNKS)), dma((3, 2, CHUNKS)),
@@ -507,7 +508,7 @@
             dma((layers, own)), dma((layers, own)),
         ],
         compiler_params=pltpu.CompilerParams(
-            collective_id=0, has_side_effects=True, vmem_limit_bytes=60 * 2**20),
+            collective_id=0, has_side_effects=True, vmem_limit_bytes=56 * 2**20),
     )(stream, doc_ids.reshape(-1, 128), norm_gain, proj_in, mix_pool, pool_gain, proj_out)
 
 

time: 181 us -> 169 us (0.934)
  Pallas kernels: 177 us -> 167 us
  local copies, waits for them, and re-layouts: 4.64 us -> 2.02 us
    pallas_call x1, Pallas kernels: 177 us -> 167 us  [body(): pl.pallas_call(functools.partial(mixer, sp, tp), out_shape=pltpu.VMEM(str...]
    unnamed x1, local copies, waits for them, and re-layouts: 4.64 us -> 2.02 us
where the time goes in v2:
time: 169 us
  Pallas kernels  167 us (99%)
  local copies, waits for them, and re-layouts  2.02 us (1%)
    pallas_call x1, Pallas kernels, body(): pl.pallas_call(functools.partial(mixer, sp, tp), out_shape=pltpu.VMEM(str...  167 us

profile of v2, /device:TPU:0, one launch (start us, length us, event | category | flops | bytes accessed | tf_op | source)
XLA Modules:
  0.0 168.8 jit_solution(2493547836363791907)
XLA Ops:
  0.0 166.7 %shard_map.73 = bf16[2048,1024]{1,0:T(8,128)(2,1)S(1)} custom-call(bf16[2048,1024]{1,0:T(8,128)(2,1)} %x_hbm.1, s32[16,128]{1,0:T(8,128)} %bitcast.1, bf16[3,4096]{1,0:T(4,128)(2,1)} %gains_ref.1, bf16[3,1024,128]{2,1,0:T(8,128)(2,1)} %win_hbm.1, bf16[3,8,128,128]{3,2,1,0:T(8,128)(2,1)} %mix_ref.1, bf16[3,1024]{1,0:T(4,128)(2,1)} %pgains_ref.1, ...), custom_call_target="tpu_custom_call" | custom-call | tf_op jit(solution)/shard_map/pallas_call | solution.py:476
  166.7 2.0 %copy.9 = bf16[2048,1024]{1,0:T(8,128)(2,1)} copy(bf16[2048,1024]{1,0:T(8,128)(2,1)S(1)} %shard_map.73) | data formatting | bytes 8388608

commit v3 on v2

--- a/solution.py
+++ b/solution.py
@@ -10,7 +10,7 @@
 EPSILON = 1e-06
 HALO = 16
 CHUNKS = 8
-EDGE = 3
+EDGE = 2
 RING = 8
 LAYERS = 3
 MESH = pl.DeviceIdType.MESH
@@ -66,7 +66,7 @@
         view = ring_view(layer, side, piece, device_at(lax.rem(origin, sp)))
         return pltpu.make_async_remote_copy(
             src_ref=view, dst_ref=view,
-            send_sem=ring_s.at[layer, side, way, turn], recv_sem=ring_r.at[layer, side, way, turn],
+            send_sem=ring_s.at[way, turn], recv_sem=ring_r.at[way, turn],
             device_id={"sp": after if way == 0 else before}, device_id_type=MESH)
 
     turns = sp - 1
@@ -81,6 +81,11 @@
                 for way in range(2):
                     ring_copy(layer, which, way, turn, 1).wait_recv()
 
+                @pl.when((turn < turns - 2) & (item > 0))
+                def _():
+                    for way in range(2):
+                        ring_copy(layer + which - 1, 1 - which, way, turn + 2, 0).wait_send()
+
                 @pl.when(turn < turns - 2)
                 def _():
                     for way in range(2):
@@ -89,6 +94,7 @@
                 @pl.when((turn >= turns - 3) & (turn < turns - 1) & (item + 1 < items))
                 def _():
                     for way in range(2):
+                        ring_copy(layer, which, way, turn - (turns - 3), 0).wait_send()
                         ring_copy(layer + which, 1 - which, way, turn - (turns - 3), 0).start()
 
     def at(i):
@@ -140,8 +146,6 @@
         return run[HALO:]
 
     def prepare():
-        for i in range(EDGE):
-            load_x(i).wait()
         for layer in range(layers):
             for side in range(2):
                 if layer + side > 0:
@@ -164,31 +168,31 @@
     def copy_sq(layer, i):
         par = lax.rem(layer, 2)
         return [pltpu.make_async_remote_copy(
-            src_ref=sq_own.at[i], dst_ref=sq_in.at[j, par, i], send_sem=sqs.at[j, i], recv_sem=sqr.at[j, par, i],
+            src_ref=sq_own.at[i], dst_ref=sq_in.at[par, i, j], send_sem=sqs.at[i], recv_sem=sqr.at[par, i],
             device_id={"tp": peer}, device_id_type=MESH)
             for j, peer in enumerate((partner, across, diagonal))]
 
     def copy1(i, lg):
         return pltpu.make_async_remote_copy(
-            src_ref=send1.at[lg, i], dst_ref=recv1.at[lg, i], send_sem=s1.at[lg, i], recv_sem=r1.at[lg, i],
+            src_ref=send1.at[lg, i], dst_ref=recv1.at[lg, i], send_sem=s1.at[i], recv_sem=r1.at[lg, i],
             device_id={"tp": partner}, device_id_type=MESH)
 
     def copy2(layer, i, lg):
         par = lax.rem(layer, 2)
         return pltpu.make_async_remote_copy(
-            src_ref=sum2.at[lg, i], dst_ref=recv2.at[par, lg, i], send_sem=s2.at[lg, i], recv_sem=r2.at[par, lg, i],
+            src_ref=sum2.at[lg, i], dst_ref=recv2.at[par, lg, i], send_sem=s2.at[i], recv_sem=r2.at[par, lg, i],
             device_id={"tp": across}, device_id_type=MESH)
 
     def copy3(i, side, lg):
         view = mixed.at[i, :, pl.ds(pl.multiple_of(side * half + lg * group, group), group)]
         return pltpu.make_async_remote_copy(
-            src_ref=view, dst_ref=view, send_sem=s3.at[lg, i], recv_sem=r3.at[lg, i],
+            src_ref=view, dst_ref=view, send_sem=s3.at[i], recv_sem=r3.at[i],
             device_id={"tp": partner}, device_id_type=MESH)
 
     def halo_copy(layer, lg):
         return pltpu.make_async_remote_copy(
             src_ref=zbuf.at[lg, pl.ds(tokens, HALO)], dst_ref=hrecv.at[layer, lg],
-            send_sem=hs.at[layer, lg], recv_sem=hr.at[layer, lg],
+            send_sem=hs.at[layer], recv_sem=hr.at[layer],
             device_id={"sp": following}, device_id_type=MESH)
 
     def groups_of(distance):
@@ -238,12 +242,18 @@
             deliver(i, high, part[:, group:])
 
     def project(layer, i):
-        gained = gained_of(layer, i)
+        @pl.when(layer > 0)
+        def _():
+            gbuf[i] = gained_of(layer, i)
+
+        gained = gbuf[i]
         other = pl.ds(pl.multiple_of((1 - core) * half, half), half)
         part = jnp.dot(gained, win[layer, :, other], preferred_element_type=F32).astype(BF16)
         for lg in range(own_groups):
-            send1[lg, i] = part[:, lg * group:(lg + 1) * group]
-            copy1(i, lg).start()
+            @pl.when((layer > 0) | ((1 - core) * own_groups + lg != s))
+            def _():
+                send1[lg, i] = part[:, lg * group:(lg + 1) * group]
+                copy1(i, lg).start()
         mine = pl.ds(pl.multiple_of(core * half, half), half)
         part = jnp.dot(gained, win[layer, :, mine], preferred_element_type=F32).astype(BF16)
         for lg in range(own_groups):
@@ -268,40 +278,32 @@
                 copy1(i, local(g)).wait_recv()
                 add_up(layer, i, local(g))
 
-            @pl.when(jnp.logical_not(owned(g)))
-            def _():
-                copy1(i, local(g)).wait_send()
         each_group(distance, act)
 
     def join(layer, i):
         for lg in range(own_groups):
-            copy1(i, lg).wait()
-            add_up(layer, i, lg)
+            @pl.when((layer > 0) | (core * own_groups + lg != s))
+            def _():
+                copy1(i, lg).wait_recv()
+                add_up(layer, i, lg)
 
     def rescale(layer, i):
         par = lax.rem(layer, 2)
+        pltpu.make_async_remote_copy(
+            src_ref=sq_in.at[par, i], dst_ref=sq_in.at[par, i], send_sem=sqs.at[i], recv_sem=sqr.at[par, i],
+            device_id={"tp": partner}, device_id_type=MESH).wait()
         total = sq_own[i]
-        for j, c in enumerate(copy_sq(layer, i)):
-            c.wait()
-            total = total + sq_in[j, par, i]
+        for j in range(3):
+            total = total + sq_in[par, i, j]
         scale_ref[i] = jnp.broadcast_to(lax.rsqrt(total / model + EPSILON), (128, rows)).T
 
     def normalise(layer, i, lg):
         par = lax.rem(layer, 2)
-        copy2(layer, i, lg).wait()
+        copy2(layer, i, lg).wait_recv()
         summed = sum2[lg, i].astype(F32) + recv2[par, lg, i].astype(F32)
         zbuf[lg, pl.ds(pl.multiple_of(HALO + i * rows, HALO), rows)] = (summed * scale_ref[i]).astype(BF16)
 
-        @pl.when(i == last)
-        def _():
-            halo_copy(layer, lg).start()
-
     def pool(layer, i, lg):
-        @pl.when(i == 0)
-        def _():
-            halo_copy(layer, lg).wait()
-            zbuf[lg, pl.ds(0, HALO)] = hrecv[layer, lg]
-
         wide_at = pl.ds(pl.multiple_of(i * rows, HALO), rows + HALO)
         pos = pos_ref[wide_at]
         z = zbuf[lg, wide_at].astype(F32)
@@ -318,10 +320,24 @@
         mixed[i, :, place_at] = (blended * pgain_ref[layer, :, lg * group:(lg + 1) * group]).astype(BF16)
         copy3(i, core, lg).start()
 
+    def side_of(i, side):
+        return mixed.at[i, :, pl.ds(pl.multiple_of(side * half, half), half)]
+
+    def take_halo(layer):
+        pltpu.make_async_remote_copy(
+            src_ref=zbuf.at[:, pl.ds(tokens, HALO)], dst_ref=hrecv.at[layer], send_sem=hs.at[layer], recv_sem=hr.at[layer],
+            device_id={"sp": following}, device_id_type=MESH).wait()
+        zbuf[:, pl.ds(0, HALO)] = hrecv[layer]
+
     def finish(layer, i):
-        for lg in range(own_groups):
-            copy3(i, core, lg).wait_send()
-            copy3(i, 1 - core, lg).wait_recv()
+        for src, dst, sems in ((send1.at[:, i], recv1.at[:, i], s1), (sum2.at[:, i], recv2.at[0, :, i], s2),
+                               (side_of(i, core), side_of(i, core), s3)):
+            pltpu.make_async_remote_copy(
+                src_ref=src, dst_ref=dst, send_sem=sems.at[i], recv_sem=r3.at[i],
+                device_id={"tp": partner}, device_id_type=MESH).wait_send()
+        pltpu.make_async_remote_copy(
+            src_ref=side_of(i, 1 - core), dst_ref=side_of(i, 1 - core), send_sem=s3.at[i], recv_sem=r3.at[i],
+            device_id={"tp": partner}, device_id_type=MESH).wait_recv()
         for j in range(2):
             cols = slice(j * (model_dev // 2), (j + 1) * (model_dev // 2))
             update = jnp.dot(mixed[i], wout[layer, :, cols], preferred_element_type=F32)
@@ -339,10 +355,15 @@
 
         @pl.loop(0, slots)
         def _(q):
-            later = layer - layer // 2
-            turn = 2 * q - q // spans + later * (15 - (q + 9) // 10) + (layer // 2) * 16
-            single = (q == spans - 1) | ((q == 0) & (layer > 0))
-            count = CHUNKS - edge
+            def past(k):
+                return (q + 15 - k) // 16
+
+            middle, final = lax.rem(layer, 2), layer // 2
+            turn = 2 * q + middle * (14 - past(4)) + final * (29 - past(2) - past(3) - past(4))
+            opening = (q == 0) & (layer > 0)
+            single = opening | ((middle == 1) & (q == 4)) | ((final == 1) & (q > 1) & (q < 5))
+            everything = ((q == 0) & (layer == 0)).astype(jnp.int32)
+            count = CHUNKS - edge + edge * everything
 
             @pl.when(live & (q < spans))
             def _():
@@ -354,6 +375,10 @@
                         def _():
                             load_x(last - j).wait()
 
+                        @pl.when(layer == 1)
+                        def _():
+                            finish(layer - 1, last - j)
+
                         gbuf[last - j] = gained_of(layer, last - j)
 
                     project_groups(layer, q, last - j)
@@ -362,41 +387,35 @@
                     def _():
                         join_groups(layer, q, last - j + 2)
 
+                    @pl.when(opening & (j == 2))
+                    def _():
+                        arrive(turn)
+
             @pl.when(q >= spans)
             def _():
                 project(layer, edge - 1 - (q - spans))
 
-            one = (q < 4) & (layer > 0)
+            one = (layer > 0) & (((ending == 1) & (q < 2)) | (live & (q > 0) & (q < 5) & (q + edge > 4)))
 
             @pl.when(one | (q > spans + 2))
             def _():
                 fresh = q // (spans + 3)
-                finish(layer - 1 + fresh, (3 - q) * (1 - fresh) + (edge - (q - spans - 3)) * fresh)
+                finish(layer - 1 + fresh, (4 - ending - q) * (1 - fresh) + (edge - (q - spans - 3)) * fresh)
 
             @pl.when(live & (q < spans))
             def _():
                 for j in range(2):
-                    join_groups(layer, q, edge + 1 - j)
+                    join_groups(layer, q, CHUNKS - count + 1 - j)
 
             @pl.when(q >= spans)
             def _():
                 join(layer, edge - 1 - (q - spans))
 
-            @pl.when(live & (turn < turns * items))
-            def _():
-                arrive(turn)
-
-            @pl.when((q == spans + 2) & live)
-            def _():
-                @pl.loop(0, CHUNKS - edge - 1)
-                def _(j):
-                    finish(layer, last - j)
-
-            second = live & (turn + 1 < turns * items) & jnp.logical_not(single)
-
-            @pl.when(second & (q == spans + 2))
-            def _():
-                arrive(turn + 1)
+            after_join = turn + opening.astype(jnp.int32)
+
+            @pl.when(live & (after_join < turns * items))
+            def _():
+                arrive(after_join)
 
             @pl.when((layer == 0) & (q == 0))
             def _():
@@ -420,6 +439,10 @@
                         @pl.when(owned(g))
                         def _():
                             normalise(layer, last - j, local(g))
+
+                            @pl.when(j == 0)
+                            def _():
+                                halo_copy(layer, local(g)).start()
                     each_group(distance, act)
 
                 @pl.loop(0, CHUNKS - edge - 1)
@@ -431,36 +454,47 @@
                                 pool(layer, last - j, lg)
                     each_group(distance, act)
 
-            old = (q < 2) & (layer > 0)
+            old = (layer > 0) & (((ending == 1) & (q < 2)) | (live & (q == 1)))
 
             @pl.when(old | (q >= spans + 2))
             def _():
                 fresh = q // (spans + 2)
                 of = layer - 1 + fresh
-                i = (1 - q) * (1 - fresh) + (edge - 1 - (q - 2 - spans)) * fresh
-                rescale(of, i)
-                for lg in range(own_groups):
-                    normalise(of, i, lg)
-
-                @pl.loop(0, 1 + (1 - fresh) * q)
+                first = (1 - q * ending) * (1 - fresh) + (edge - 1 - (q - 2 - spans)) * fresh
+
+                @pl.loop(0, 1 + (1 - fresh) * (1 - ending))
                 def _(j):
+                    i = first - j
+                    rescale(of, i)
+
+                    @pl.when(i == 0)
+                    def _():
+                        take_halo(of)
+
                     for lg in range(own_groups):
-                        pool(of, i + 1 - j, lg)
-
-            @pl.when(second & (q != spans + 2))
+                        normalise(of, i, lg)
+                        pool(of, i + 1, lg)
+
+                        @pl.when(i == 0)
+                        def _():
+                            pool(of, i, lg)
+
+            @pl.when(live & (turn + 1 < turns * items) & jnp.logical_not(single))
             def _():
                 arrive(turn + 1)
+
+            @pl.when((layer > 0) & live & (q == slots - 1))
+            def _():
+                @pl.loop(0, CHUNKS - edge - 1)
+                def _(j):
+                    finish(layer, last - j)
 
     for i in range(2):
         finish(layers - 1, 1 - i)
 
-    @pl.loop(0, layers)
-    def _(layer):
-        for side in range(2):
-            for way in range(2):
-                @pl.loop(0, turns)
-                def _(turn):
-                    ring_copy(layer, side, way, turn, 0).wait_send()
+    for way in range(2):
+        for turn in range(turns):
+            ring_copy(layers - 1, 1, way, turn, 0).wait_send()
 
 
 def body(sp, tp, stream, doc_ids, norm_gain, proj_in, mix_pool, pool_gain, proj_out):
@@ -491,7 +525,7 @@
             vmem((own, HALO + tokens, group), BF16),
             vmem((layers, own, HALO, group), BF16),
             vmem((CHUNKS, 1, rows), F32),
-            vmem((3, 2, CHUNKS, 1, rows), F32),
+            vmem((2, CHUNKS, 3, 1, rows), F32),
             vmem((CHUNKS, rows, 128), F32),
             vmem((2 * HALO + tokens, 128), F32),
             vmem((2 * HALO, 128), F32),
@@ -500,12 +534,12 @@
             vmem((layers, 1, half), F32),
             dma((CHUNKS,)), dma((layers, 2)),
             dma, dma,
-            dma((layers, 2, 2, sp - 1)), dma((layers, 2, 2, sp - 1)),
-            dma((3, CHUNKS)), dma((3, 2, CHUNKS)),
-            dma((own, CHUNKS)), dma((own, CHUNKS)),
-            dma((own, CHUNKS)), dma((2, own, CHUNKS)),
-            dma((own, CHUNKS)), dma((own, CHUNKS)),
-            dma((layers, own)), dma((layers, own)),
+            dma((2, sp - 1)), dma((2, sp - 1)),
+            dma((CHUNKS,)), dma((2, CHUNKS)),
+            dma((CHUNKS,)), dma((own, CHUNKS)),
+            dma((CHUNKS,)), dma((2, own, CHUNKS)),
+            dma((CHUNKS,)), dma((CHUNKS,)),
+            dma((layers,)), dma((layers,)),
         ],
         compiler_params=pltpu.CompilerParams(
             collective_id=0, has_side_effects=True, vmem_limit_bytes=56 * 2**20),

time: 169 us -> 159 us (0.941)
  Pallas kernels: 167 us -> 156 us
    pallas_call x1, Pallas kernels: 167 us -> 156 us  [body(): pl.pallas_call(functools.partial(mixer, sp, tp), out_shape=pltpu.VMEM(str...]
where the time goes in v3:
time: 159 us
  Pallas kernels  156 us (98%)
  local copies, waits for them, and re-layouts  2.02 us (1%)
    pallas_call x1, Pallas kernels, body(): pl.pallas_call(functools.partial(mixer, sp, tp), out_shape=pltpu.VMEM(str...  156 us

profile of v3, /device:TPU:0, one launch (start us, length us, event | category | flops | bytes accessed | tf_op | source)
XLA Modules:
  0.0 158.5 jit_solution(6031622377843084233)
XLA Ops:
  0.0 156.5 %shard_map.73 = bf16[2048,1024]{1,0:T(8,128)(2,1)S(1)} custom-call(bf16[2048,1024]{1,0:T(8,128)(2,1)} %x_hbm.1, s32[16,128]{1,0:T(8,128)} %bitcast.1, bf16[3,4096]{1,0:T(4,128)(2,1)} %gains_ref.1, bf16[3,1024,128]{2,1,0:T(8,128)(2,1)} %win_hbm.1, bf16[3,8,128,128]{3,2,1,0:T(8,128)(2,1)} %mix_ref.1, bf16[3,1024]{1,0:T(4,128)(2,1)} %pgains_ref.1, ...), custom_call_target="tpu_custom_call" | custom-call | tf_op jit(solution)/shard_map/pallas_call | solution.py:510
  156.5 2.0 %copy.9 = bf16[2048,1024]{1,0:T(8,128)(2,1)} copy(bf16[2048,1024]{1,0:T(8,128)(2,1)S(1)} %shard_map.73) | data formatting | bytes 8388608

commit v4 on v3

--- a/solution.py
+++ b/solution.py
@@ -19,8 +19,8 @@
 
 def mixer(sp, tp, x_hbm, doc_ref, gains_ref, win_hbm, mix_ref, pgains_ref, wout_hbm, h,
           win, wout, gbuf, send1, own1, recv1, sum2, recv2, mixed, zbuf, hrecv,
-          sq_own, sq_in, scale_ref, labels, before_labels, pos_ref, gain_ref, pgain_ref,
-          xs, ws, ls, lr, ring_s, ring_r, sqs, sqr, s1, r1, s2, r2, s3, r3, hs, hr):
+          sq_own, sq_in, scale_ref, labels, before_labels, pos_ref, inverse, gain_ref, pgain_ref,
+          xs, ws, ls, lr, ring_s, ring_r, sqs, sqr, s1, r1, s2, r2, rh, s3, r3, hs, hr):
     layers, model_dev, chan_dev = win_hbm.shape
     tokens = h.shape[0]
     rows = tokens // CHUNKS
@@ -123,10 +123,12 @@
     for peer in peers:
         pl.semaphore_signal(barrier, inc=1, device_id=peer, device_id_type=MESH)
     own_gain = gains_ref[:, pl.ds(pl.multiple_of(t * model_dev, model_dev), model_dev)].astype(F32)
-    own_pgain = pgains_ref[:, pl.ds(pl.multiple_of(core * half, half), half)].astype(F32)
     for layer in range(layers):
         gain_ref[layer] = own_gain[layer:layer + 1]
-        pgain_ref[layer] = own_pgain[layer:layer + 1]
+    for lg in range(own_groups):
+        own_pgain = pgains_ref[:, columns(lg + own_groups * lax.rem(lg + core, 2))].astype(F32)
+        for layer in range(layers):
+            pgain_ref[layer, :, lg * group:(lg + 1) * group] = own_pgain[layer:layer + 1]
     load_w(0, 0).wait()
     pl.semaphore_wait(barrier, len(peers))
     for turn in range(2):
@@ -162,8 +164,10 @@
 
         @pl.loop(0, CHUNKS)
         def _(i):
-            pos_ref[pl.ds(pl.multiple_of(HALO + i * rows, HALO), rows)] = distances(
-                labels[pl.ds(pl.multiple_of(HALO + i * rows, HALO), rows + HALO)])
+            pos = distances(labels[pl.ds(pl.multiple_of(HALO + i * rows, HALO), rows + HALO)])
+            pos_ref[pl.ds(pl.multiple_of(HALO + i * rows, HALO), rows)] = pos
+            for w in range(4):
+                inverse[w, at(i)] = 1.0 / jnp.minimum(pos + 1.0, float(2 ** (1 + w)))
 
     def copy_sq(layer, i):
         par = lax.rem(layer, 2)
@@ -183,8 +187,23 @@
             src_ref=sum2.at[lg, i], dst_ref=recv2.at[par, lg, i], send_sem=s2.at[i], recv_sem=r2.at[par, lg, i],
             device_id={"tp": across}, device_id_type=MESH)
 
+    def copy_part(lg, part):
+        par = (layers - 1) % 2
+        cut = pl.ds(part * (rows // 2), rows // 2)
+        return pltpu.make_async_remote_copy(
+            src_ref=sum2.at[lg, 0, cut], dst_ref=recv2.at[par, lg, 0, cut],
+            send_sem=s2.at[0], recv_sem=r2.at[par, lg, 0] if part else rh.at[lg],
+            device_id={"tp": across}, device_id_type=MESH)
+
+    def normalise_part(lg, part):
+        par = (layers - 1) % 2
+        cut = pl.ds(part * (rows // 2), rows // 2)
+        copy_part(lg, part).wait_recv()
+        summed = sum2[lg, 0, cut].astype(F32) + recv2[par, lg, 0, cut].astype(F32)
+        zbuf[lg, pl.ds(HALO + part * (rows // 2), rows // 2)] = (summed * scale_ref[0, cut]).astype(BF16)
+
     def copy3(i, side, lg):
-        view = mixed.at[i, :, pl.ds(pl.multiple_of(side * half + lg * group, group), group)]
+        view = mixed.at[i, :, columns(group_at(side, lg))]
         return pltpu.make_async_remote_copy(
             src_ref=view, dst_ref=view, send_sem=s3.at[i], recv_sem=r3.at[i],
             device_id={"tp": partner}, device_id_type=MESH)
@@ -195,11 +214,17 @@
             send_sem=hs.at[layer], recv_sem=hr.at[layer],
             device_id={"sp": following}, device_id_type=MESH)
 
+    def group_at(side, lg):
+        return lg + own_groups * lax.rem(lg + side, 2)
+
+    def columns_of(layer, side):
+        return jnp.concatenate([win[layer, :, columns(group_at(side, lg))] for lg in range(own_groups)], axis=1)
+
     def groups_of(distance):
         return (device_at(lax.rem(here - distance + sp, sp)), device_at(lax.rem(here + distance, sp)))
 
     def owned(g):
-        return g // own_groups == core
+        return lax.rem(g // own_groups + g, 2) == core
 
     def local(g):
         return lax.rem(g, own_groups)
@@ -217,51 +242,57 @@
         return gained
 
     def deliver(i, g, value):
+        several = value.shape[0] // rows
+
         @pl.when(owned(g))
         def _():
-            own1[local(g), i] = value
+            for k in range(several):
+                own1[local(g), i + k] = value[k * rows:(k + 1) * rows]
 
         @pl.when(jnp.logical_not(owned(g)))
         def _():
-            send1[local(g), i] = value
-            copy1(i, local(g)).start()
-
-    def project_groups(layer, distance, i):
+            for k in reversed(range(several)):
+                send1[local(g), i + k] = value[k * rows:(k + 1) * rows]
+                copy1(i + k, local(g)).start()
+
+    def project_groups(layer, distance, i, several):
         low, high = groups_of(distance)
+        span = pl.ds(pl.multiple_of(i * rows, rows), several * rows)
 
         @pl.when(lax.rem(distance, sp // 2) == 0)
         def _():
-            part = jnp.dot(gbuf[i], win[layer, :, columns(low)], preferred_element_type=F32).astype(BF16)
+            part = jnp.dot(gbuf[span], win[layer, :, columns(low)], preferred_element_type=F32).astype(BF16)
             deliver(i, low, part)
 
         @pl.when(lax.rem(distance, sp // 2) > 0)
         def _():
             weights = jnp.concatenate([win[layer, :, columns(low)], win[layer, :, columns(high)]], axis=1)
-            part = jnp.dot(gbuf[i], weights, preferred_element_type=F32).astype(BF16)
+            part = jnp.dot(gbuf[span], weights, preferred_element_type=F32).astype(BF16)
             deliver(i, low, part[:, :group])
             deliver(i, high, part[:, group:])
 
     def project(layer, i):
         @pl.when(layer > 0)
         def _():
-            gbuf[i] = gained_of(layer, i)
-
-        gained = gbuf[i]
-        other = pl.ds(pl.multiple_of((1 - core) * half, half), half)
-        part = jnp.dot(gained, win[layer, :, other], preferred_element_type=F32).astype(BF16)
+            gbuf[at(i)] = gained_of(layer, i)
+
+        gained = gbuf[at(i)]
+        part = jnp.dot(gained, columns_of(layer, 1 - core), preferred_element_type=F32).astype(BF16)
         for lg in range(own_groups):
-            @pl.when((layer > 0) | ((1 - core) * own_groups + lg != s))
+            @pl.when((layer > 0) | (group_at(1 - core, lg) != s))
             def _():
                 send1[lg, i] = part[:, lg * group:(lg + 1) * group]
                 copy1(i, lg).start()
-        mine = pl.ds(pl.multiple_of(core * half, half), half)
-        part = jnp.dot(gained, win[layer, :, mine], preferred_element_type=F32).astype(BF16)
+        part = jnp.dot(gained, columns_of(layer, core), preferred_element_type=F32).astype(BF16)
         for lg in range(own_groups):
             own1[lg, i] = part[:, lg * group:(lg + 1) * group]
 
     def add_up(layer, i, lg):
         sum2[lg, i] = (own1[lg, i].astype(F32) + recv1[lg, i].astype(F32)).astype(BF16)
-        copy2(layer, i, lg).start()
+
+        @pl.when((layer < layers - 1) | (i > 0))
+        def _():
+            copy2(layer, i, lg).start()
 
     def each_group(distance, act):
         low, high = groups_of(distance)
@@ -282,10 +313,16 @@
 
     def join(layer, i):
         for lg in range(own_groups):
-            @pl.when((layer > 0) | (core * own_groups + lg != s))
+            @pl.when((layer > 0) | (group_at(core, lg) != s))
             def _():
                 copy1(i, lg).wait_recv()
                 add_up(layer, i, lg)
+
+        @pl.when((layer == layers - 1) & (i == 0))
+        def _():
+            for part in (1, 0):
+                for lg in range(own_groups):
+                    copy_part(lg, part).start()
 
     def rescale(layer, i):
         par = lax.rem(layer, 2)
@@ -313,11 +350,9 @@
         while size < window:
             total = total + jnp.where(pos >= size, pltpu.roll(total, size, 0), 0.0)
             size *= 2
-        count = jnp.minimum(pos[HALO:] + 1.0, float(window))
-        pooled = (total[HALO:] / count - z[HALO:]).astype(BF16)
-        blended = jnp.dot(pooled, mix_ref[layer, core * own_groups + lg], preferred_element_type=F32)
-        place_at = pl.ds(pl.multiple_of(core * half + lg * group, group), group)
-        mixed[i, :, place_at] = (blended * pgain_ref[layer, :, lg * group:(lg + 1) * group]).astype(BF16)
+        pooled = (total[HALO:] * inverse[lg % 4, at(i)] - z[HALO:]).astype(BF16)
+        blended = jnp.dot(pooled, mix_ref[layer, group_at(core, lg)], preferred_element_type=F32)
+        mixed[i, :, columns(group_at(core, lg))] = (blended * pgain_ref[layer, :, lg * group:(lg + 1) * group]).astype(BF16)
         copy3(i, core, lg).start()
 
     def side_of(i, side):
@@ -351,7 +386,7 @@
         edge = EDGE + layer
         ending = layer // layers
         live = layer < layers
-        slots = (spans + edge) * (1 - ending) + 2 * ending
+        slots = (spans + edge) * (1 - ending) + ending
 
         @pl.loop(0, slots)
         def _(q):
@@ -359,37 +394,61 @@
                 return (q + 15 - k) // 16
 
             middle, final = lax.rem(layer, 2), layer // 2
-            turn = 2 * q + middle * (14 - past(4)) + final * (29 - past(2) - past(3) - past(4))
+            turn = 2 * q + middle * (14 - past(4)) + final * (28 - past(3) - past(4) - past(7))
             opening = (q == 0) & (layer > 0)
-            single = opening | ((middle == 1) & (q == 4)) | ((final == 1) & (q > 1) & (q < 5))
+            single = opening | ((middle == 1) & (q == 4)) | ((final == 1) & ((q == 3) | (q == 4) | (q == 7)))
             everything = ((q == 0) & (layer == 0)).astype(jnp.int32)
             count = CHUNKS - edge + edge * everything
 
+            inline = ((q == 0) | ((q == 1) & (layer == 0))).astype(jnp.int32)
+
+            def gain(i):
+                @pl.when(layer == 0)
+                def _():
+                    load_x(i).wait()
+
+                @pl.when(layer == 1)
+                def _():
+                    finish(layer - 1, i)
+
+                gbuf[at(i)] = gained_of(layer, i)
+
             @pl.when(live & (q < spans))
             def _():
-                @pl.loop(0, count)
+                @pl.loop(0, count // 2)
                 def _(j):
                     @pl.when(q == 0)
                     def _():
-                        @pl.when(layer == 0)
-                        def _():
-                            load_x(last - j).wait()
-
-                        @pl.when(layer == 1)
-                        def _():
-                            finish(layer - 1, last - j)
-
-                        gbuf[last - j] = gained_of(layer, last - j)
-
-                    project_groups(layer, q, last - j)
-
-                    @pl.when(j >= 2)
+                        @pl.loop(0, 2)
+                        def _(k):
+                            gain(last - 2 * j - k)
+
+                    project_groups(layer, q, last - 2 * j - 1, 2)
+
+                    early = opening & (final == 1) & (j == 0)
+
+                    @pl.when(early)
                     def _():
-                        join_groups(layer, q, last - j + 2)
-
-                    @pl.when(opening & (j == 2))
+                        @pl.loop(0, 2)
+                        def _(k):
+                            finish(layer - 1, last - 2 - k)
+
+                    @pl.when(early | ((inline == 1) & (j > 0) & ((final == 0) | (q > 0))))
                     def _():
-                        arrive(turn)
+                        for k in range(2):
+                            join_groups(layer, q, last - 2 * j + 2 - 2 * early.astype(jnp.int32) - k)
+
+                    @pl.when(opening & (((middle == 1) & (j == 0)) | (j == 1)))
+                    def _():
+                        arrive(turn + j)
+
+                @pl.when(lax.rem(count, 2) == 1)
+                def _():
+                    @pl.when(q == 0)
+                    def _():
+                        gain(CHUNKS - count)
+
+                    project_groups(layer, q, CHUNKS - count, 1)
 
             @pl.when(q >= spans)
             def _():
@@ -397,25 +456,35 @@
 
             one = (layer > 0) & (((ending == 1) & (q < 2)) | (live & (q > 0) & (q < 5) & (q + edge > 4)))
 
-            @pl.when(one | (q > spans + 2))
-            def _():
-                fresh = q // (spans + 3)
-                finish(layer - 1 + fresh, (4 - ending - q) * (1 - fresh) + (edge - (q - spans - 3)) * fresh)
+            @pl.when(one)
+            def _():
+                finish(layer - 1, 4 - ending - q)
 
             @pl.when(live & (q < spans))
             def _():
-                for j in range(2):
-                    join_groups(layer, q, CHUNKS - count + 1 - j)
+                joined = (count // 2 - 1) * 2 * inline
+
+                @pl.loop(joined, count)
+                def _(j):
+                    join_groups(layer, q, last - j)
 
             @pl.when(q >= spans)
             def _():
                 join(layer, edge - 1 - (q - spans))
 
-            after_join = turn + opening.astype(jnp.int32)
-
-            @pl.when(live & (after_join < turns * items))
-            def _():
-                arrive(after_join)
+            @pl.when(live & (turn < turns * items) & jnp.logical_not(opening))
+            def _():
+                arrive(turn)
+
+            @pl.when((layer > 0) & live & (q == slots - 1))
+            def _():
+                @pl.loop(0, 2 + 2 * final)
+                def _(j):
+                    finish(layer, last - j)
+
+            more = live & (turn + 1 < turns * items) & jnp.logical_not(single)
+            lag = 3 - (layer + 9) // 10
+            reps = 1 + ((layer == 0) & (q == slots - 1)).astype(jnp.int32)
 
             @pl.when((layer == 0) & (q == 0))
             def _():
@@ -424,35 +493,6 @@
             @pl.when((layer == 0) & (q == 1))
             def _():
                 measure()
-
-            @pl.when(live & (q > 1) & (q < spans + 2))
-            def _():
-                distance = q - 2
-
-                @pl.loop(0, CHUNKS - edge)
-                def _(j):
-                    @pl.when(distance == 0)
-                    def _():
-                        rescale(layer, last - j)
-
-                    def act(g):
-                        @pl.when(owned(g))
-                        def _():
-                            normalise(layer, last - j, local(g))
-
-                            @pl.when(j == 0)
-                            def _():
-                                halo_copy(layer, local(g)).start()
-                    each_group(distance, act)
-
-                @pl.loop(0, CHUNKS - edge - 1)
-                def _(j):
-                    def act(g):
-                        for lg in range(own_groups):
-                            @pl.when(owned(g) & (local(g) == lg))
-                            def _():
-                                pool(layer, last - j, lg)
-                    each_group(distance, act)
 
             old = (layer > 0) & (((ending == 1) & (q < 2)) | (live & (q == 1)))
 
@@ -479,18 +519,51 @@
                         def _():
                             pool(of, i, lg)
 
-            @pl.when(live & (turn + 1 < turns * items) & jnp.logical_not(single))
-            def _():
-                arrive(turn + 1)
-
-            @pl.when((layer > 0) & live & (q == slots - 1))
-            def _():
-                @pl.loop(0, CHUNKS - edge - 1)
-                def _(j):
-                    finish(layer, last - j)
-
-    for i in range(2):
-        finish(layers - 1, 1 - i)
+            @pl.loop(0, reps)
+            def _(rep):
+                @pl.when(live & (q >= lag) & (q < spans + lag))
+                def _():
+                    distance = q - lag + rep
+
+                    @pl.loop(0, CHUNKS - edge)
+                    def _(j):
+                        @pl.when(distance == 0)
+                        def _():
+                            rescale(layer, last - j)
+
+                        def act(g):
+                            @pl.when(owned(g))
+                            def _():
+                                normalise(layer, last - j, local(g))
+
+                                @pl.when(j == 0)
+                                def _():
+                                    halo_copy(layer, local(g)).start()
+                        each_group(distance, act)
+
+                    @pl.loop(0, CHUNKS - edge - 1)
+                    def _(j):
+                        def act(g):
+                            for lg in range(own_groups):
+                                @pl.when(owned(g) & (local(g) == lg))
+                                def _():
+                                    pool(layer, last - j, lg)
+                        each_group(distance, act)
+
+                @pl.when(more & (rep == reps - 1))
+                def _():
+                    arrive(turn + 1)
+
+    rescale(layers - 1, 0)
+    take_halo(layers - 1)
+    for i in (1, 0):
+        for lg in range(own_groups):
+            normalise_part(lg, i)
+            pool(layers - 1, i, lg)
+
+        @pl.loop(0, 2 - i)
+        def _(j):
+            finish(layers - 1, 1 + i - j)
 
     for way in range(2):
         for turn in range(turns):
@@ -515,7 +588,7 @@
         scratch_shapes=[
             vmem((layers, model_dev, channels), BF16),
             vmem((layers, channels, model_dev), BF16),
-            vmem((CHUNKS, rows, model_dev), BF16),
+            vmem((tokens, model_dev), BF16),
             vmem((own, CHUNKS, rows, group), BF16),
             vmem((own, CHUNKS, rows, group), BF16),
             vmem((own, CHUNKS, rows, group), BF16),
@@ -530,6 +603,7 @@
             vmem((2 * HALO + tokens, 128), F32),
             vmem((2 * HALO, 128), F32),
             vmem((HALO + tokens, 128), F32),
+            vmem((4, tokens, 128), F32),
             vmem((layers, 1, model_dev), F32),
             vmem((layers, 1, half), F32),
             dma((CHUNKS,)), dma((layers, 2)),
@@ -537,7 +611,7 @@
             dma((2, sp - 1)), dma((2, sp - 1)),
             dma((CHUNKS,)), dma((2, CHUNKS)),
             dma((CHUNKS,)), dma((own, CHUNKS)),
-            dma((CHUNKS,)), dma((2, own, CHUNKS)),
+            dma((CHUNKS,)), dma((2, own, CHUNKS)), dma((own,)),
             dma((CHUNKS,)), dma((CHUNKS,)),
             dma((layers,)), dma((layers,)),
         ],

time: 159 us -> 158 us (level)
  no operation moved by 1% of the time
where the time goes in v4:
time: 158 us; the launch traced here: 157 us
  Pallas kernels  155 us (98%)
  local copies, waits for them, and re-layouts  2.02 us (1%)
    pallas_call x1, Pallas kernels, body(): pl.pallas_call(functools.partial(mixer, sp, tp), out_shape=pltpu.VMEM(str...  155 us

profile of v4, /device:TPU:0, one launch (start us, length us, event | category | flops | bytes accessed | tf_op | source)
XLA Modules:
  0.0 157.4 jit_solution(3034806179480826600)
XLA Ops:
  0.0 155.4 %shard_map.73 = bf16[2048,1024]{1,0:T(8,128)(2,1)S(1)} custom-call(bf16[2048,1024]{1,0:T(8,128)(2,1)} %x_hbm.1, s32[16,128]{1,0:T(8,128)} %bitcast.1, bf16[3,4096]{1,0:T(4,128)(2,1)} %gains_ref.1, bf16[3,1024,128]{2,1,0:T(8,128)(2,1)} %win_hbm.1, bf16[3,8,128,128]{3,2,1,0:T(8,128)(2,1)} %mix_ref.1, bf16[3,1024]{1,0:T(4,128)(2,1)} %pgains_ref.1, ...), custom_call_target="tpu_custom_call" | custom-call | tf_op jit(solution)/shard_map/pallas_call | solution.py:583
  155.4 2.0 %copy.9 = bf16[2048,1024]{1,0:T(8,128)(2,1)} copy(bf16[2048,1024]{1,0:T(8,128)(2,1)S(1)} %shard_map.73) | data formatting | bytes 8388608

commit v5 on v4

--- a/solution.py
+++ b/solution.py
@@ -423,6 +423,11 @@
                         def _(k):
                             gain(last - 2 * j - k)
 
+                    @pl.when((middle == 1) & (q == 0) & (j > 0))
+                    def _():
+                        for k in range(2):
+                            join_groups(layer, q, last - 2 * j + 2 - k)
+
                     project_groups(layer, q, last - 2 * j - 1, 2)
 
                     early = opening & (final == 1) & (j == 0)
@@ -433,7 +438,7 @@
                         def _(k):
                             finish(layer - 1, last - 2 - k)
 
-                    @pl.when(early | ((inline == 1) & (j > 0) & ((final == 0) | (q > 0))))
+                    @pl.when(early | ((inline == 1) & (j > 0) & (layer == 0)))
                     def _():
                         for k in range(2):
                             join_groups(layer, q, last - 2 * j + 2 - 2 * early.astype(jnp.int32) - k)
@@ -454,6 +459,12 @@
             def _():
                 project(layer, edge - 1 - (q - spans))
 
+            @pl.when(live & (q < spans) & (inline == 0))
+            def _():
+                @pl.loop(0, count - 2)
+                def _(j):
+                    join_groups(layer, q, last - j)
+
             one = (layer > 0) & (((ending == 1) & (q < 2)) | (live & (q > 0) & (q < 5) & (q + edge > 4)))
 
             @pl.when(one)
@@ -462,7 +473,7 @@
 
             @pl.when(live & (q < spans))
             def _():
-                joined = (count // 2 - 1) * 2 * inline
+                joined = (count // 2 - 1) * 2 * inline + (count - 2) * (1 - inline)
 
                 @pl.loop(joined, count)
                 def _(j):

time: 158 us -> 158 us (level)
  no operation moved by 1% of the time
where the time goes in v5:
time: 158 us; the launch traced here: 157 us
  Pallas kernels  155 us (98%)
  local copies, waits for them, and re-layouts  2.02 us (1%)
    pallas_call x1, Pallas kernels, body(): pl.pallas_call(functools.partial(mixer, sp, tp), out_shape=pltpu.VMEM(str...  155 us

profile of v5, /device:TPU:0, one launch (start us, length us, event | category | flops | bytes accessed | tf_op | source)
XLA Modules:
  0.0 157.5 jit_solution(5566182031641858312)
XLA Ops:
  0.0 155.5 %shard_map.73 = bf16[2048,1024]{1,0:T(8,128)(2,1)S(1)} custom-call(bf16[2048,1024]{1,0:T(8,128)(2,1)} %x_hbm.1, s32[16,128]{1,0:T(8,128)} %bitcast.1, bf16[3,4096]{1,0:T(4,128)(2,1)} %gains_ref.1, bf16[3,1024,128]{2,1,0:T(8,128)(2,1)} %win_hbm.1, bf16[3,8,128,128]{3,2,1,0:T(8,128)(2,1)} %mix_ref.1, bf16[3,1024]{1,0:T(4,128)(2,1)} %pgains_ref.1, ...), custom_call_target="tpu_custom_call" | custom-call | tf_op jit(solution)/shard_map/pallas_call | solution.py:594
  155.5 2.0 %copy.9 = bf16[2048,1024]{1,0:T(8,128)(2,1)} copy(bf16[2048,1024]{1,0:T(8,128)(2,1)S(1)} %shard_map.73) | data formatting | bytes 8388608
